TPU v7x, 128 devices: a whole 4x4x4 slice. The times are simulated.
128 devices in a mesh: sp: 32 (over z, y, core), tp: 4 (over x).
Axes of the slice: x: 4, y: 4, z: 4, core: 2. Of those that a mesh axis runs over, the one named last changes fastest.
Arguments:
- tokens: bfloat16 [4, 2048, 1024], P(None, 'sp', 'tp'), may hold values from -6 to 6
- norm_gain: float32 [4, 1024], replicated, may hold values from 0.1 to 1.9
- val_weight: bfloat16 [4, 1024, 512], P(None, 'sp', 'tp'), may hold values from -0.1875 to 0.1875
- gate_weight: bfloat16 [4, 1024, 512], P(None, 'sp', 'tp'), may hold values from -0.1875 to 0.1875
- conv_taps: float32 [4, 31, 512], P(None, None, 'tp'), may hold values from -1 to 1
- conv_bias: float32 [4, 512], P(None, 'tp'), may hold values from -3 to 3
- ln_gain: float32 [4, 512], P(None, 'tp'), may hold values from 0.1 to 1.9
- ln_shift: float32 [4, 512], P(None, 'tp'), may hold values from -3 to 3
- out_weight: bfloat16 [4, 512, 1024], P(None, 'tp', 'sp'), may hold values from -0.25 to 0.25
Outputs:
- stream: bfloat16 [4, 2048, 1024], P(None, 'sp', 'tp')
All inputs are finite; a program needn't handle non-finite values.
Results may differ from a plain program's by a relative error of at most 0.02.
Values may be sent and summed in bfloat16 or wider, within the bound.
A program may use at most 64 MiB of HBM per device.

v0:
```python
from functools import partial

import jax
import jax.numpy as jnp
from jax import lax
from jax.sharding import PartitionSpec as P

LAYERS = 4


epsilon = 1e-06


def over_all(shard, axis, dim, absorb, state):
    everything = jax.tree.map(lambda a: lax.all_gather(a, axis, axis=dim, tiled=True), shard)
    return absorb(state, everything, jnp.int32(0))


def with_halo(shard, sides, width, wrap):
    for axis, dim in sides:
        size, length = lax.axis_size(axis), shard.shape[dim]
        up = [(i, (i + 1) % size) for i in range(size if wrap else size - 1)]
        down = [(j, i) for i, j in up]
        last = lax.slice_in_dim(shard, length - width, length, axis=dim)
        initial = lax.slice_in_dim(shard, 0, width, axis=dim)
        before = lax.ppermute(last, axis, up)
        after = lax.ppermute(initial, axis, down)
        shard = jnp.concatenate([before, shard, after], axis=dim)
    return shard


def together(arrays, axis):
    ends = [0]
    for a in arrays:
        ends.append(ends[-1] + a.size)
    subtotal = lax.psum(jnp.concatenate([a.ravel() for a in arrays]), axis)
    return tuple(subtotal[b:e].reshape(a.shape) for a, b, e in zip(arrays, ends, ends[1:]))


def on_whole(shard, axis, dim, work):
    return work(lax.all_gather(shard, axis, axis=dim, tiled=True), jnp.int32(0))


def depthwise(padded, tap_weights, length):
    running = padded[:, 0:length] * tap_weights[0]
    for tap_idx in range(1, tap_weights.shape[0]):
        running = running + padded[:, tap_idx : tap_idx + length] * tap_weights[tap_idx]
    return running


def add_rows(left_rows, running, shard_piece, offset):
    columns = lax.dynamic_slice_in_dim(left_rows, offset, shard_piece.shape[0], 1)
    return running + jnp.dot(columns, shard_piece, preferred_element_type=jnp.float32)


def add_both(left_rows, totals, pieces, offset):
    return (
        add_rows(left_rows, totals[0], pieces[0], offset),
        add_rows(left_rows, totals[1], pieces[1], offset),
    )


def project_rows(left_rows, shard_piece, offset):
    return jnp.dot(left_rows, shard_piece, preferred_element_type=jnp.float32)


def shards(
    tokens, norm_gain, val_weight, gate_weight, conv_taps, conv_bias, ln_gain, ln_shift, out_weight
):
    stream = tokens
    num_seqs = tokens.shape[0]
    local_len = tokens.shape[1]
    chan_width = val_weight.shape[2]
    all_channels = chan_width * lax.axis_size("tp")
    half_width = conv_taps.shape[1] // 2
    for layer_idx in range(LAYERS):
        gathered = lax.all_gather(stream, "tp", axis=2, tiled=True)
        widened = gathered.astype(jnp.float32)
        scaled = widened * lax.rsqrt(jnp.mean(widened * widened, axis=-1, keepdims=True) + epsilon)
        normed = (scaled * norm_gain[layer_idx]).astype(jnp.bfloat16)
        tok_rows = normed.reshape(-1, normed.shape[2])
        zeroed = jnp.zeros((tok_rows.shape[0], chan_width), jnp.float32)
        values, gates = over_all(
            (val_weight[layer_idx], gate_weight[layer_idx]),
            "sp",
            0,
            partial(add_both, tok_rows),
            (zeroed, zeroed),
        )
        gated = (
            (values * jax.nn.sigmoid(gates))
            .astype(jnp.bfloat16)
            .reshape(num_seqs, local_len, chan_width)
        )
        padded = with_halo(gated, (("sp", 1),), half_width, False)
        convolved = (
            depthwise(padded.astype(jnp.float32), conv_taps[layer_idx], local_len)
            + conv_bias[layer_idx]
        )
        first_sum, second_sum = together(
            (jnp.sum(convolved, axis=-1), jnp.sum(convolved * convolved, axis=-1)), "tp"
        )
        mean_val = (first_sum / all_channels)[..., None]
        spread = (second_sum / all_channels)[..., None] - mean_val * mean_val
        centered = convolved - mean_val
        normalized = (
            centered * lax.rsqrt(spread + epsilon) * ln_gain[layer_idx] + ln_shift[layer_idx]
        )
        activated = jax.nn.silu(normalized).astype(jnp.bfloat16).reshape(-1, chan_width)
        partial_terms = on_whole(out_weight[layer_idx], "sp", 1, partial(project_rows, activated))
        full_width = partial_terms.shape[1]
        summed = lax.psum_scatter(
            partial_terms.reshape(num_seqs, local_len, full_width).astype(jnp.bfloat16),
            "tp",
            scatter_dimension=2,
            tiled=True,
        ).astype(jnp.float32)
        stream = (stream.astype(jnp.float32) + summed).astype(jnp.bfloat16)
    return stream


def solution(mesh):
    return jax.shard_map(
        shards,
        mesh=mesh,
        in_specs=(
            P(None, "sp", "tp"),
            P(),
            P(None, "sp", "tp"),
            P(None, "sp", "tp"),
            P(None, None, "tp"),
            P(None, "tp"),
            P(None, "tp"),
            P(None, "tp"),
            P(None, "tp", "sp"),
        ),
        out_specs=P(None, "sp", "tp"),
        check_vma=False,
    )
```

profile of v0, /device:TPU:1, one launch (start us, length us, event | category | flops | bytes accessed | tf_op | source)
XLA Modules:
  0.0 451.9 jit_solution(18299880186058381866)
XLA Ops:
  7.4 12.5 %all_gather.48 = bf16[4,64,1024]{2,1,0:T(8,128)(2,1)S(1)} all-gather(bf16[4,64,256]{2,1,0:T(8,128)(2,1)} %param.9), channel_id=1, replica_groups=mesh['sp'=32,'tp'=4] {'tp'}, dimensions={2}, use_global_device_ids=true | all-gather | bytes 655360 | tf_op jit(solution)/shard_map/all_gather | solution.py:77
  20.7 28.5 %all-gather = bf16[1,1024,128]{2,1,0:T(8,128)(2,1)S(1)} all-gather(bf16[1,32,128]{2,1,0:T(8,128)(2,1)S(1)} %get-tuple-element.155), channel_id=2, replica_groups=mesh['sp'=32,'tp'=4] {'sp'}, dimensions={1}, use_global_device_ids=true | all-gather | bytes 270336 | tf_op jit(solution)/shard_map/all_gather | solution.py:15
  49.2 24.1 %all-gather.1 = bf16[1,1024,128]{2,1,0:T(8,128)(2,1)S(1)} all-gather(bf16[1,32,128]{2,1,0:T(8,128)(2,1)S(1)} %get-tuple-element.151), channel_id=3, replica_groups=mesh['sp'=32,'tp'=4] {'sp'}, dimensions={1}, use_global_device_ids=true | all-gather | bytes 270336 | tf_op jit(solution)/shard_map/all_gather | solution.py:15
  79.9 25.7 %all-gather.2 = bf16[1,128,1024]{1,2,0:T(8,128)(2,1)S(1)} all-gather(bf16[1,128,32]{1,2,0:T(8,128)(2,1)S(1)} %get-tuple-element.157), channel_id=4, replica_groups=mesh['sp'=32,'tp'=4] {'sp'}, dimensions={2}, use_global_device_ids=true | all-gather | bytes 270336 | tf_op jit(solution)/shard_map/all_gather | solution.py:41
  106.4 8.7 %psum.28 = f32[512]{0:T(512)S(1)} all-reduce(f32[512]{0:T(512)S(1)} %pad_maximum_fusion), channel_id=1, replica_groups=mesh['sp'=32,'tp'=4] {'tp'}, use_global_device_ids=true, to_apply=%region_3.0 | all-reduce | flops 512 | bytes 4096 | tf_op jit(solution)/shard_map/psum | solution.py:36
  116.5 24.9 %all-gather.3 = bf16[1,1024,128]{2,1,0:T(8,128)(2,1)S(1)} all-gather(bf16[1,32,128]{2,1,0:T(8,128)(2,1)S(1)} %get-tuple-element.154), channel_id=5, replica_groups=mesh['sp'=32,'tp'=4] {'sp'}, dimensions={1}, use_global_device_ids=true | all-gather | bytes 270336 | tf_op jit(solution)/shard_map/all_gather | solution.py:15
  141.4 23.7 %all-gather.4 = bf16[1,1024,128]{2,1,0:T(8,128)(2,1)S(1)} all-gather(bf16[1,32,128]{2,1,0:T(8,128)(2,1)S(1)} %get-tuple-element.150), channel_id=6, replica_groups=mesh['sp'=32,'tp'=4] {'sp'}, dimensions={1}, use_global_device_ids=true | all-gather | bytes 270336 | tf_op jit(solution)/shard_map/all_gather | solution.py:15
  166.1 10.3 %all_gather.52 = bf16[4,64,1024]{2,1,0:T(8,128)(2,1)S(1)} all-gather(bf16[4,64,256]{2,1,0:T(8,128)(2,1)S(1)} %add_convert_fusion.3), channel_id=1, replica_groups=mesh['sp'=32,'tp'=4] {'tp'}, dimensions={2}, use_global_device_ids=true | all-gather | bytes 655360 | tf_op jit(solution)/shard_map/all_gather | solution.py:77
  177.4 5.0 %collective-permute-start.2 = (bf16[4,15,128]{2,1,0:T(8,128)(2,1)S(1)}, bf16[4,15,128]{2,1,0:T(8,128)(2,1)S(1)}, u32[]{:S(2)}, u32[]{:S(2)}) collective-permute-start(bf16[4,15,128]{2,1,0:T(8,128)(2,1)S(1)} %get-tuple-element.21), channel_id=1, source_target_pairs={{0,4},{4,8},{8,12},{12,16},{16,20},{20,24},{24,28},{28,32},{32,36}... | collective-permute-start | bytes 46088 | tf_op jit(solution)/shard_map/ppermute | solution.py:26
  184.3 27.1 %all-gather.5 = bf16[1,128,1024]{1,2,0:T(8,128)(2,1)S(1)} all-gather(bf16[1,128,32]{1,2,0:T(8,128)(2,1)S(1)} %get-tuple-element.158), channel_id=7, replica_groups=mesh['sp'=32,'tp'=4] {'sp'}, dimensions={2}, use_global_device_ids=true | all-gather | bytes 270336 | tf_op jit(solution)/shard_map/all_gather | solution.py:41
  212.2 6.0 %psum.29 = f32[512]{0:T(512)S(1)} all-reduce(f32[512]{0:T(512)S(1)} %pad_maximum_fusion.1), channel_id=1, replica_groups=mesh['sp'=32,'tp'=4] {'tp'}, use_global_device_ids=true, to_apply=%region_8.9 | all-reduce | flops 512 | bytes 4096 | tf_op jit(solution)/shard_map/psum | solution.py:36
  219.6 24.1 %all-gather.6 = bf16[1,1024,128]{2,1,0:T(8,128)(2,1)S(1)} all-gather(bf16[1,32,128]{2,1,0:T(8,128)(2,1)S(1)} %get-tuple-element.156), channel_id=8, replica_groups=mesh['sp'=32,'tp'=4] {'sp'}, dimensions={1}, use_global_device_ids=true | all-gather | bytes 270336 | tf_op jit(solution)/shard_map/all_gather | solution.py:15
  243.7 24.1 %all-gather.7 = bf16[1,1024,128]{2,1,0:T(8,128)(2,1)S(1)} all-gather(bf16[1,32,128]{2,1,0:T(8,128)(2,1)S(1)} %get-tuple-element.152), channel_id=9, replica_groups=mesh['sp'=32,'tp'=4] {'sp'}, dimensions={1}, use_global_device_ids=true | all-gather | bytes 270336 | tf_op jit(solution)/shard_map/all_gather | solution.py:15
  268.8 10.3 %all_gather.56 = bf16[4,64,1024]{2,1,0:T(8,128)(2,1)S(1)} all-gather(bf16[4,64,256]{2,1,0:T(8,128)(2,1)S(1)} %add_convert_fusion.2), channel_id=1, replica_groups=mesh['sp'=32,'tp'=4] {'tp'}, dimensions={2}, use_global_device_ids=true | all-gather | bytes 655360 | tf_op jit(solution)/shard_map/all_gather | solution.py:77
  280.1 3.8 collective-permute-start.4
  286.1 26.7 %all-gather.8 = bf16[1,128,1024]{1,2,0:T(8,128)(2,1)S(1)} all-gather(bf16[1,128,32]{1,2,0:T(8,128)(2,1)S(1)} %get-tuple-element.160), channel_id=10, replica_groups=mesh['sp'=32,'tp'=4] {'sp'}, dimensions={2}, use_global_device_ids=true | all-gather | bytes 270336 | tf_op jit(solution)/shard_map/all_gather | solution.py:41
  313.5 7.9 %psum.30 = f32[512]{0:T(512)S(1)} all-reduce(f32[512]{0:T(512)S(1)} %pad_maximum_fusion.2), channel_id=1, replica_groups=mesh['sp'=32,'tp'=4] {'tp'}, use_global_device_ids=true, to_apply=%region_13.14 | all-reduce | flops 512 | bytes 4096 | tf_op jit(solution)/shard_map/psum | solution.py:36
  322.9 24.9 %all-gather.9 = bf16[1,1024,128]{2,1,0:T(8,128)(2,1)S(1)} all-gather(bf16[1,32,128]{2,1,0:T(8,128)(2,1)S(1)} %get-tuple-element.153), channel_id=11, replica_groups=mesh['sp'=32,'tp'=4] {'sp'}, dimensions={1}, use_global_device_ids=true | all-gather | bytes 270336 | tf_op jit(solution)/shard_map/all_gather | solution.py:15
  347.8 23.8 %all-gather.10 = bf16[1,1024,128]{2,1,0:T(8,128)(2,1)S(1)} all-gather(bf16[1,32,128]{2,1,0:T(8,128)(2,1)S(1)} %get-tuple-element.149), channel_id=12, replica_groups=mesh['sp'=32,'tp'=4] {'sp'}, dimensions={1}, use_global_device_ids=true | all-gather | bytes 270336 | tf_op jit(solution)/shard_map/all_gather | solution.py:15
  372.5 10.3 %all_gather.60 = bf16[4,64,1024]{2,1,0:T(8,128)(2,1)S(1)} all-gather(bf16[4,64,256]{2,1,0:T(8,128)(2,1)S(1)} %add_convert_fusion.1), channel_id=1, replica_groups=mesh['sp'=32,'tp'=4] {'tp'}, dimensions={2}, use_global_device_ids=true | all-gather | bytes 655360 | tf_op jit(solution)/shard_map/all_gather | solution.py:77
  383.8 5.0 %collective-permute-start.6 = (bf16[4,15,128]{2,1,0:T(8,128)(2,1)S(1)}, bf16[4,15,128]{2,1,0:T(8,128)(2,1)S(1)}, u32[]{:S(2)}, u32[]{:S(2)}) collective-permute-start(bf16[4,15,128]{2,1,0:T(8,128)(2,1)S(1)} %get-tuple-element.17), channel_id=1, source_target_pairs={{0,4},{4,8},{8,12},{12,16},{16,20},{20,24},{24,28},{28,32},{32,36}... | collective-permute-start | bytes 46088 | tf_op jit(solution)/shard_map/ppermute | solution.py:26
  390.8 26.9 %all-gather.11 = bf16[1,128,1024]{1,2,0:T(8,128)(2,1)S(1)} all-gather(bf16[1,128,32]{1,2,0:T(8,128)(2,1)S(1)} %get-tuple-element.159), channel_id=13, replica_groups=mesh['sp'=32,'tp'=4] {'sp'}, dimensions={2}, use_global_device_ids=true | all-gather | bytes 270336 | tf_op jit(solution)/shard_map/all_gather | solution.py:41
  418.5 6.0 %psum.31 = f32[512]{0:T(512)S(1)} all-reduce(f32[512]{0:T(512)S(1)} %pad_maximum_fusion.3), channel_id=1, replica_groups=mesh['sp'=32,'tp'=4] {'tp'}, use_global_device_ids=true, to_apply=%region_18.19 | all-reduce | flops 512 | bytes 4096 | tf_op jit(solution)/shard_map/psum | solution.py:36
  425.8 18.0 %reduce-scatter.11.cloned.1.call-done = bf16[4,64,256]{2,1,0:T(8,128)(2,1)} async-done(((bf16[4,64,1024]{2,1,0:T(8,128)(2,1)}), bf16[4,64,256]{2,1,0:T(8,128)(2,1)}) %reduce-scatter.11.cloned.1.call-update) | async-done | bytes 131088 | tf_op jit(solution)/shard_map/reduce_scatter | solution.py:112
  (121 shorter events, 30.3 us)
Async XLA Ops:
  6.5 158.6 %reduce-scatter.5.cloned.1.call-start = ((), (), s32[]{:S(2)}) async-start(), calls=%async_computation.4 | async-start | bytes 655360 | tf_op jit(solution)/shard_map/reduce_scatter | solution.py:112
  19.9 0.8 copy-start.2
  20.7 28.5 %copy-start.3 = (bf16[4,32,128]{2,1,0:T(8,128)(2,1)S(1)}, bf16[4,32,128]{2,1,0:T(8,128)(2,1)}, u32[]{:S(2)}) copy-start(bf16[4,32,128]{2,1,0:T(8,128)(2,1)} %param.12) | copy-start | bytes 98308
  74.1 4.4 copy-start.1
  74.1 5.1 %copy-start.4 = (bf16[4,128,32]{1,2,0:T(8,128)(2,1)S(1)}, bf16[4,128,32]{1,2,0:T(8,128)(2,1)}, u32[]{:S(2)}) copy-start(bf16[4,128,32]{1,2,0:T(8,128)(2,1)} %param.17) | copy-start | bytes 98308
  74.1 31.5 %collective-permute-start = (bf16[4,15,128]{2,1,0:T(8,128)(2,1)S(1)}, bf16[4,15,128]{2,1,0:T(8,128)(2,1)S(1)}, u32[]{:S(2)}, u32[]{:S(2)}) collective-permute-start(bf16[4,15,128]{2,1,0:T(8,128)(2,1)S(1)} %get-tuple-element.23), channel_id=1, source_target_pairs={{0,4},{4,8},{8,12},{12,16},{16,20},{20,24},{24,28},{28,32},{32,36}... | collective-permute-start | bytes 46088 | tf_op jit(solution)/shard_map/ppermute | solution.py:26
  76.0 29.6 %collective-permute-start.1 = (bf16[4,15,128]{2,1,0:T(8,128)(2,1)S(1)}, bf16[4,15,128]{2,1,0:T(8,128)(2,1)S(1)}, u32[]{:S(2)}, u32[]{:S(2)}) collective-permute-start(bf16[4,15,128]{2,1,0:T(8,128)(2,1)S(1)} %get-tuple-element.24), channel_id=1, source_target_pairs={{4,0},{8,4},{12,8},{16,12},{20,16},{24,20},{28,24},{32,28},{36,32}... | collective-permute-start | bytes 46088 | tf_op jit(solution)/shard_map/ppermute | solution.py:27
  78.5 0.7 copy-start.5
  79.2 0.7 copy-start.6
  79.2 0.7 copy-start.7
  116.4 151.4 %reduce-scatter.7.cloned.1.call-start = ((), (), s32[]{:S(2)}) async-start(), calls=%async_computation.5 | async-start | bytes 655360 | tf_op jit(solution)/shard_map/reduce_scatter | solution.py:112
  141.4 23.7 %copy-start = (bf16[4,64,256]{2,1,0:T(8,128)(2,1)S(1)}, bf16[4,64,256]{2,1,0:T(8,128)(2,1)}, u32[]{:S(2)}) copy-start(bf16[4,64,256]{2,1,0:T(8,128)(2,1)} %param.9) | copy-start | bytes 393220
  177.4 34.0 %collective-permute-start.2 = (bf16[4,15,128]{2,1,0:T(8,128)(2,1)S(1)}, bf16[4,15,128]{2,1,0:T(8,128)(2,1)S(1)}, u32[]{:S(2)}, u32[]{:S(2)}) collective-permute-start(bf16[4,15,128]{2,1,0:T(8,128)(2,1)S(1)} %get-tuple-element.21), channel_id=1, source_target_pairs={{0,4},{4,8},{8,12},{12,16},{16,20},{20,24},{24,28},{28,32},{32,36}... | collective-permute-start | bytes 46088 | tf_op jit(solution)/shard_map/ppermute | solution.py:26
  182.4 29.0 %collective-permute-start.3 = (bf16[4,15,128]{2,1,0:T(8,128)(2,1)S(1)}, bf16[4,15,128]{2,1,0:T(8,128)(2,1)S(1)}, u32[]{:S(2)}, u32[]{:S(2)}) collective-permute-start(bf16[4,15,128]{2,1,0:T(8,128)(2,1)S(1)} %get-tuple-element.22), channel_id=1, source_target_pairs={{4,0},{8,4},{12,8},{16,12},{20,16},{24,20},{28,24},{32,28},{36,32}... | collective-permute-start | bytes 46088 | tf_op jit(solution)/shard_map/ppermute | solution.py:27
  219.5 152.0 %reduce-scatter.9.cloned.1.call-start = ((), (), s32[]{:S(2)}) async-start(), calls=%async_computation.6 | async-start | bytes 655360 | tf_op jit(solution)/shard_map/reduce_scatter | solution.py:112
  280.1 32.6 %collective-permute-start.4 = (bf16[4,15,128]{2,1,0:T(8,128)(2,1)S(1)}, bf16[4,15,128]{2,1,0:T(8,128)(2,1)S(1)}, u32[]{:S(2)}, u32[]{:S(2)}) collective-permute-start(bf16[4,15,128]{2,1,0:T(8,128)(2,1)S(1)} %get-tuple-element.19), channel_id=1, source_target_pairs={{0,4},{4,8},{8,12},{12,16},{16,20},{20,24},{24,28},{28,32},{32,36}... | collective-permute-start | bytes 46088 | tf_op jit(solution)/shard_map/ppermute | solution.py:26
  283.9 28.9 %collective-permute-start.5 = (bf16[4,15,128]{2,1,0:T(8,128)(2,1)S(1)}, bf16[4,15,128]{2,1,0:T(8,128)(2,1)S(1)}, u32[]{:S(2)}, u32[]{:S(2)}) collective-permute-start(bf16[4,15,128]{2,1,0:T(8,128)(2,1)S(1)} %get-tuple-element.20), channel_id=1, source_target_pairs={{4,0},{8,4},{12,8},{16,12},{20,16},{24,20},{28,24},{32,28},{36,32}... | collective-permute-start | bytes 46088 | tf_op jit(solution)/shard_map/ppermute | solution.py:27
  322.8 121.0 %reduce-scatter.11.cloned.1.call-start = ((), (), s32[]{:S(2)}) async-start(), calls=%async_computation.7 | async-start | bytes 655360 | tf_op jit(solution)/shard_map/reduce_scatter | solution.py:112
  383.8 33.9 %collective-permute-start.6 = (bf16[4,15,128]{2,1,0:T(8,128)(2,1)S(1)}, bf16[4,15,128]{2,1,0:T(8,128)(2,1)S(1)}, u32[]{:S(2)}, u32[]{:S(2)}) collective-permute-start(bf16[4,15,128]{2,1,0:T(8,128)(2,1)S(1)} %get-tuple-element.17), channel_id=1, source_target_pairs={{0,4},{4,8},{8,12},{12,16},{16,20},{20,24},{24,28},{28,32},{32,36}... | collective-permute-start | bytes 46088 | tf_op jit(solution)/shard_map/ppermute | solution.py:26
  388.8 28.9 %collective-permute-start.7 = (bf16[4,15,128]{2,1,0:T(8,128)(2,1)S(1)}, bf16[4,15,128]{2,1,0:T(8,128)(2,1)S(1)}, u32[]{:S(2)}, u32[]{:S(2)}) collective-permute-start(bf16[4,15,128]{2,1,0:T(8,128)(2,1)S(1)} %get-tuple-element.18), channel_id=1, source_target_pairs={{4,0},{8,4},{12,8},{16,12},{20,16},{24,20},{28,24},{32,28},{36,32}... | collective-permute-start | bytes 46088 | tf_op jit(solution)/shard_map/ppermute | solution.py:27
Sparse Core Ops, SparseCore 0:
  116.6 17.4 reduce-scatter.4
  219.7 17.8 reduce-scatter.6
  322.9 17.4 reduce-scatter.8
  425.9 17.8 reduce-scatter.10
where the time goes:
time: 455 us; the launch traced here: 452 us
  blocking collectives  376 us (83%)
  starting transfers between devices  24.3 us (5%)
  waiting for transfers between devices  18.1 us (4%)
  between operations  13.5 us (3%)
  other arithmetic  8.4 us (2%)
  matrix products  7 us (2%)
    all_gather x8, blocking collectives, over_all(): lax.all_gather(a, axis, axis=dim, tiled=True)  198 us
    all_gather x4, blocking collectives, on_whole(): return work(lax.all_gather(shard, axis, axis=dim, tiled=True), jnp.int32(0))  106 us
    all_gather x4, blocking collectives, shards(): gathered = lax.all_gather(stream, 'tp', axis=2, tiled=True)  43.3 us
    psum x4, blocking collectives, together(): subtotal = lax.psum(jnp.concatenate([a.ravel() for a in arrays]), axis)  28.6 us
    reduce_scatter x4, waiting for transfers between devices, shards(): lax.psum_scatter(partial_terms.reshape(num_seqs, local_len, full_width).a...  18 us
    ppermute x4, starting transfers between devices, with_halo(): before = lax.ppermute(last, axis, up)  15.7 us
  transfers between devices with their start and end apart: 12, of which 1 were waited for; matrix products, arithmetic and copies ran while one was open for 0% of the time, Pallas kernels for 0%

commit v1 on v0

v1 whole, which is shorter than its diff:
```python
import jax
import jax.numpy as jnp
from jax import lax
from jax.sharding import PartitionSpec as P

LAYERS = 4
EPSILON = 1e-06
STEP = 16


def shards(
    tokens, norm_gain, val_weight, gate_weight, conv_taps, conv_bias, ln_gain, ln_shift, out_weight
):
    sp = lax.axis_index("sp")
    size = lax.axis_size("sp")
    length = tokens.shape[1]
    taps = conv_taps.shape[1]
    half = taps // 2
    own = lax.all_to_all(tokens, "tp", 0, 2, tiled=True)[0]
    up = [(i, (i + 1) % size) for i in range(size)]
    down = [(j, i) for i, j in up]
    before = lax.ppermute(own, "sp", up)
    after = lax.ppermute(own, "sp", down)
    stream = jnp.concatenate([before, own, after], axis=0)

    def whole(w, dim):
        w = lax.all_gather(w, "sp", axis=dim, tiled=True)
        return lax.all_gather(w, "tp", axis=3 - dim, tiled=True)

    small = lax.all_gather(
        jnp.concatenate([conv_taps, conv_bias[:, None], ln_gain[:, None], ln_shift[:, None]], axis=1),
        "tp", axis=2, tiled=True,
    )
    vals, gates, outs = whole(val_weight, 1), whole(gate_weight, 1), whole(out_weight, 2)
    position = sp * length - length + jnp.arange(3 * length)
    inside = (position >= 0) & (position < size * length)
    low = 0
    for layer in range(LAYERS):
        rows = stream.shape[0]
        widened = stream.astype(jnp.float32)
        scaled = widened * lax.rsqrt(jnp.mean(widened * widened, axis=-1, keepdims=True) + EPSILON)
        normed = (scaled * norm_gain[layer]).astype(jnp.bfloat16)
        values = jnp.dot(normed, vals[layer], preferred_element_type=jnp.float32)
        gate = jnp.dot(normed, gates[layer], preferred_element_type=jnp.float32)
        gated = (values * jax.nn.sigmoid(gate)).astype(jnp.bfloat16)
        gated = jnp.where(inside[low : low + rows, None], gated, 0).astype(jnp.float32)
        keep = rows - 2 * STEP
        first = STEP - half
        running = gated[first : first + keep] * small[layer, 0]
        for k in range(1, taps):
            running = running + gated[first + k : first + k + keep] * small[layer, k]
        convolved = running + small[layer, taps]
        mean = jnp.mean(convolved, axis=-1, keepdims=True)
        centered = convolved - mean
        spread = jnp.mean(centered * centered, axis=-1, keepdims=True)
        normalized = centered * lax.rsqrt(spread + EPSILON) * small[layer, taps + 1] + small[layer, taps + 2]
        activated = jax.nn.silu(normalized).astype(jnp.bfloat16)
        branch = jnp.dot(activated, outs[layer], preferred_element_type=jnp.float32)
        stream = (widened[STEP : STEP + keep] + branch).astype(jnp.bfloat16)
        low += STEP
    return lax.all_to_all(stream[None], "tp", 2, 0, tiled=True)


def solution(mesh):
    return jax.shard_map(
        shards,
        mesh=mesh,
        in_specs=(
            P(None, "sp", "tp"),
            P(),
            P(None, "sp", "tp"),
            P(None, "sp", "tp"),
            P(None, None, "tp"),
            P(None, "tp"),
            P(None, "tp"),
            P(None, "tp"),
            P(None, "tp", "sp"),
        ),
        out_specs=P(None, "sp", "tp"),
        check_vma=False,
    )
```

time: 455 us -> 336 us (0.74)
  blocking collectives: 376 us -> 21.3 us
  waiting for transfers between devices: 18.1 us -> 267 us
  starting transfers between devices: 24.3 us -> 7.9 us
    all_gather x16 -> x1, blocking collectives: 348 us -> 13 us  [shards(): lax.all_gather(jnp.concatenate([conv_taps, conv_bias[:, None], ln_gain[:,...]
    all_gather x0 -> x6, waiting for transfers between devices: none -> 262 us  [the longest x3 136 us: whole(): w = lax.all_gather(w, 'sp', axis=dim, tiled=True)]
    psum x4 -> x0, blocking collectives: 28.6 us -> none  [together(): subtotal = lax.psum(jnp.concatenate([a.ravel() for a in arrays]), axis)]
    ppermute x8 -> x2, starting transfers between devices: 24.1 us -> 3.73 us  [the longest x1 2.97 us: shards(): after = lax.ppermute(own, 'sp', down)]
    reduce_scatter x4 -> x0, waiting for transfers between devices: 18 us -> none  [shards(): lax.psum_scatter(partial_terms.reshape(num_seqs, local_len, full_width).a...]
    all_to_all x0 -> x1, blocking collectives: none -> 8.3 us  [shards(): return lax.all_to_all(stream[None], 'tp', 2, 0, tiled=True)]
    convert_element_type x12 -> x1, other arithmetic: 5.28 us -> 0.08 us  [shards(): widened = stream.astype(jnp.float32)]
  transfers between devices with their start and end apart: 12 -> 9, of which waited for: 1 -> 7; matrix products, arithmetic and copies ran while one was open for 0% -> 2% of each run, Pallas kernels for 0% -> 0%
where the time goes in v1:
time: 336 us; the launch traced here: 334 us
  waiting for transfers between devices  267 us (79%)
  blocking collectives  21.3 us (6%)
  between operations  13.8 us (4%)
  matrix products  10.7 us (3%)
  starting transfers between devices  7.9 us (2%)
  other arithmetic  7.6 us (2%)
  local copies, waits for them, and re-layouts  5.73 us (2%)
    all_gather x3, waiting for transfers between devices, whole(): w = lax.all_gather(w, 'sp', axis=dim, tiled=True)  136 us
    all_gather x3, waiting for transfers between devices, whole(): return lax.all_gather(w, 'tp', axis=3 - dim, tiled=True)  126 us
    all_gather x1, blocking collectives, shards(): lax.all_gather(jnp.concatenate([conv_taps, conv_bias[:, None], ln_gain[:,...  13 us
    all_to_all x1, blocking collectives, shards(): return lax.all_to_all(stream[None], 'tp', 2, 0, tiled=True)  8.3 us
  transfers between devices with their start and end apart: 9, of which 7 were waited for; matrix products, arithmetic and copies ran while one was open for 2% of the time, Pallas kernels for 0%

profile of v1, /device:TPU:1, one launch (start us, length us, event | category | flops | bytes accessed | tf_op | source)
XLA Modules:
  0.0 333.8 jit_solution(2352190466711751897)
XLA Ops:
  6.5 0.7 all-gather.11.cloned.1.call-update
  7.3 0.7 all-gather.7.cloned.1.call-update
  8.8 47.3 %all-gather.11.cloned.1.call-done = bf16[4,1024,128]{2,1,0:T(8,128)(2,1)} async-done(((bf16[4,32,128]{2,1,0:T(8,128)(2,1)}), bf16[4,1024,128]{2,1,0:T(8,128)(2,1)}) %all-gather.11.cloned.1.call-update) | async-done | bytes 1048592 | tf_op jit(solution)/shard_map/all_gather | solution.py:27
  56.2 44.4 %all-gather.7.cloned.1.call-done = bf16[4,1024,128]{2,1,0:T(8,128)(2,1)} async-done(((bf16[4,32,128]{2,1,0:T(8,128)(2,1)}), bf16[4,1024,128]{2,1,0:T(8,128)(2,1)}) %all-gather.7.cloned.1.call-update) | async-done | bytes 1048592 | tf_op jit(solution)/shard_map/all_gather | solution.py:27
  100.6 44.4 %all-gather.15.cloned.1.call-done = bf16[4,128,1024]{1,2,0:T(8,128)(2,1)} async-done(((bf16[4,128,32]{1,2,0:T(8,128)(2,1)}), bf16[4,128,1024]{1,2,0:T(8,128)(2,1)}) %all-gather.15.cloned.1.call-update) | async-done | bytes 1048592 | tf_op jit(solution)/shard_map/all_gather | solution.py:27
  145.0 4.0 %all-to-all-start = ((bf16[4,64,256]{2,1,0:T(8,128)(2,1)}), bf16[4,64,256]{2,1,0:T(8,128)(2,1)S(1)}, u32[]{:S(2)}, u32[]{:S(2)}) async-start(bf16[4,64,256]{2,1,0:T(8,128)(2,1)} %param.9), calls=%async_computation | async-start | bytes 262144 | tf_op jit(solution)/shard_map/all_to_all | solution.py:19
  149.0 0.9 pad_maximum_fusion
  149.9 13.0 %all_gather.25 = f32[4,34,512]{2,0,1:T(4,128)S(1)} all-gather(f32[4,34,128]{2,0,1:T(4,128)S(1)} %pad_maximum_fusion), channel_id=1, replica_groups=mesh['sp'=32,'tp'=4] {'tp'}, dimensions={2}, use_global_device_ids=true | all-gather | bytes 348160 | tf_op jit(solution)/shard_map/all_gather | solution.py:30
  162.9 0.9 fusion.201
  164.5 3.0 collective-permute-start.1
  167.4 0.8 collective-permute-start
  168.2 2.9 collective-permute-done.1
  171.4 26.1 %all-gather.13.cloned.1.call-done = bf16[4,1024,512]{2,1,0:T(8,128)(2,1)} async-done(((bf16[4,1024,128]{2,1,0:T(8,128)(2,1)}), bf16[4,1024,512]{2,1,0:T(8,128)(2,1)}) %all-gather.13.cloned.1.call-update) | async-done | bytes 4194320 | tf_op jit(solution)/shard_map/all_gather | solution.py:28
  197.5 1.7 fusion.4
  199.3 49.7 %all-gather.9.cloned.1.call-done = bf16[4,1024,512]{2,1,0:T(8,128)(2,1)} async-done(((bf16[4,1024,128]{2,1,0:T(8,128)(2,1)}), bf16[4,1024,512]{2,1,0:T(8,128)(2,1)}) %all-gather.9.cloned.1.call-update) | async-done | bytes 4194320 | tf_op jit(solution)/shard_map/all_gather | solution.py:28
  248.9 1.7 fusion.17
  250.6 1.4 fusion.191
  252.3 50.0 %all-gather.17.cloned.1.call-done = bf16[4,512,1024]{1,2,0:T(8,128)(2,1)} async-done(((bf16[4,128,1024]{1,2,0:T(8,128)(2,1)}), bf16[4,512,1024]{1,2,0:T(8,128)(2,1)}) %all-gather.17.cloned.1.call-update) | async-done | bytes 4194320 | tf_op jit(solution)/shard_map/all_gather | solution.py:28
  302.3 2.0 multiply_reduce_fusion.1
  304.3 1.7 fusion.7
  306.4 0.8 fusion.189
  307.4 1.2 copy-done.1
  314.8 2.3 reduce
  317.3 8.3 %all_to_all.33 = bf16[4,2,8192]{2,1,0:T(2,128)(2,1)S(1)} all-to-all(bf16[4,2,8192]{2,1,0:T(2,128)(2,1)S(1)} %reshape.227), channel_id=1, replica_groups=mesh['sp'=32,'tp'=4] {'tp'}, dimensions={0} | all-to-all | bytes 262144 | tf_op jit(solution)/shard_map/all_to_all | solution.py:61
  (66 shorter events, 10.4 us)
Async XLA Ops:
  6.5 49.6 %all-gather.11.cloned.1.call-start = ((), (), s32[]{:S(2)}) async-start(), calls=%async_computation.4 | async-start | bytes 1081344 | tf_op jit(solution)/shard_map/all_gather | solution.py:27
  7.3 93.3 %all-gather.7.cloned.1.call-start = ((), (), s32[]{:S(2)}) async-start(), calls=%async_computation.2 | async-start | bytes 1081344 | tf_op jit(solution)/shard_map/all_gather | solution.py:27
  8.0 137.0 %all-gather.15.cloned.1.call-start = ((), (), s32[]{:S(2)}) async-start(), calls=%async_computation.6 | async-start | bytes 1081344 | tf_op jit(solution)/shard_map/all_gather | solution.py:27
  8.7 188.8 %all-gather.13.cloned.1.call-start = ((), (), s32[]{:S(2)}) async-start(), calls=%async_computation.5 | async-start | bytes 5242880 | tf_op jit(solution)/shard_map/all_gather | solution.py:28
  56.1 192.8 %all-gather.9.cloned.1.call-start = ((), (), s32[]{:S(2)}) async-start(), calls=%async_computation.3 | async-start | bytes 5242880 | tf_op jit(solution)/shard_map/all_gather | solution.py:28
  100.6 201.7 %all-gather.17.cloned.1.call-start = ((), (), s32[]{:S(2)}) async-start(), calls=%async_computation.7 | async-start | bytes 5242880 | tf_op jit(solution)/shard_map/all_gather | solution.py:28
  145.0 19.3 %all-to-all-start = ((bf16[4,64,256]{2,1,0:T(8,128)(2,1)}), bf16[4,64,256]{2,1,0:T(8,128)(2,1)S(1)}, u32[]{:S(2)}, u32[]{:S(2)}) async-start(bf16[4,64,256]{2,1,0:T(8,128)(2,1)} %param.9), calls=%async_computation | async-start | bytes 262144 | tf_op jit(solution)/shard_map/all_to_all | solution.py:19
  164.5 6.7 %collective-permute-start.1 = (bf16[64,1024]{1,0:T(8,128)(2,1)S(1)}, bf16[64,1024]{1,0:T(8,128)(2,1)S(1)}, u32[]{:S(2)}, u32[]{:S(2)}) collective-permute-start(bf16[64,1024]{1,0:T(8,128)(2,1)S(1)} %bitcast.202), channel_id=1, source_target_pairs={{4,0},{8,4},{12,8},{16,12},{20,16},{24,20},{28,24},{32,28},{36,32}... | collective-permute-start | bytes 393224 | tf_op jit(solution)/shard_map/ppermute | solution.py:23
  167.4 3.7 %collective-permute-start = (bf16[64,1024]{1,0:T(8,128)(2,1)S(1)}, bf16[64,1024]{1,0:T(8,128)(2,1)S(1)}, u32[]{:S(2)}, u32[]{:S(2)}) collective-permute-start(bf16[64,1024]{1,0:T(8,128)(2,1)S(1)} %bitcast.203), channel_id=1, source_target_pairs={{0,4},{4,8},{8,12},{12,16},{16,20},{20,24},{24,28},{28,32},{32,36}... | collective-permute-start | bytes 393224 | tf_op jit(solution)/shard_map/ppermute | solution.py:22
  302.3 3.7 %copy-start = (bf16[4,1024,512]{2,1,0:T(8,128)(2,1)S(1)}, bf16[4,1024,512]{2,1,0:T(8,128)(2,1)}, u32[]{:S(2)}) copy-start(bf16[4,1024,512]{2,1,0:T(8,128)(2,1)} %all-gather.9.cloned.1.call-done) | copy-start | bytes 12582916
  306.4 2.2 copy-start.1
  307.2 2.9 copy-start.2
Sparse Core Ops, SparseCore 0:
  9.5 46.5 all-gather.10
  58.3 42.2 all-gather.6
  102.7 42.2 all-gather.14
  146.5 50.9 all-gather.12
  199.0 49.8 all-gather.8
  250.4 51.7 all-gather.16

commit v2 on v1

v2 whole, which is shorter than its diff:
```python
import functools

import jax
import jax.numpy as jnp
from jax import lax
from jax.experimental import pallas as pl
from jax.experimental.pallas import tpu as pltpu
from jax.sharding import PartitionSpec as P

LAYERS = 4
EPSILON = 1e-06
STEP = 16
TAPS = 31
MESH = pl.DeviceIdType.MESH
F32, BF16 = jnp.float32, jnp.bfloat16
ORDERS = (("x", "y", "z"), ("y", "z", "x"), ("z", "x", "y"))
GROUPS = ((0, 1), (1, 3))
CHUNK = 32


def wrap(v, n):
    return lax.rem(v + n, n)


def kernel(
    tok, gain, val, gate, taps, bias, lng, lnb, outw, out,
    W, ow, ost, X, Y, N, V, G, GT, CV, A, O, gainv, T, S,
    loc, s1, r1, s2, r2, s3, r3, sd, rd, st, rt, sh, rh, sp_, rp_, so, ro,
):
    sp = lax.axis_index("sp")
    x = lax.axis_index("tp")
    n_sp = 32
    c = lax.rem(sp, 2)
    y = lax.rem(sp // 2, 4)
    z = sp // 8
    me = {"x": x, "y": y, "z": z}

    def device(d, step):
        at = dict(me)
        at[d] = wrap(me[d] + step, 4)
        return ((at["z"] * 4 + at["y"]) * 2 + c, at["x"])

    partner = (sp + 1 - 2 * c, x)
    left, right = (wrap(sp - 1, n_sp), x), (wrap(sp + 1, n_sp), x)
    across = (wrap(sp + 1 - 2 * (1 - c), n_sp), x)
    x_peers = [(sp, wrap(x + k, 4)) for k in (1, 2, 3)]

    cols = lambda i, w: pl.ds(pl.multiple_of(i * w, w), w)
    starts = [
        pltpu.make_async_copy(val, W.at[:, 0, z, y, c, :, cols(x, 128)], loc.at[0]),
        pltpu.make_async_copy(gate, W.at[:, 1, z, y, c, :, cols(x, 128)], loc.at[1]),
        pltpu.make_async_copy(outw, ow, loc.at[2]),
        pltpu.make_async_copy(tok.at[x], X.at[pl.ds(64, 64), cols(x, 256)], loc.at[3]),
        pltpu.make_async_copy(gain, gainv, loc.at[4]),
        pltpu.make_async_copy(taps, T.at[x], loc.at[5]),
        pltpu.make_async_copy(bias, S.at[x, 0], loc.at[6]),
        pltpu.make_async_copy(lng, S.at[x, 1], loc.at[7]),
        pltpu.make_async_copy(lnb, S.at[x, 2], loc.at[8]),
    ]
    for copy in starts:
        copy.start()

    barrier = pltpu.get_barrier_semaphore()
    peers = x_peers + [device("y", 1), device("y", -1), device("z", 1), device("z", -1), partner, across]
    for peer in peers:
        pl.semaphore_signal(barrier, inc=1, device_id=peer, device_id_type=MESH)

    starts[2].wait()
    eye = (
        lax.broadcasted_iota(jnp.int32, (32, 32), 0) == lax.broadcasted_iota(jnp.int32, (32, 32), 1)
    ).astype(BF16)
    for l in range(LAYERS):
        ost[l] = lax.dot_general(
            eye, ow[l], (((1,), (1,)), ((), ())), preferred_element_type=F32
        ).astype(BF16)
    place = pltpu.make_async_copy(ost, W.at[:, 2, z, y, c, :, cols(x, 128)], loc.at[9])
    place.start()
    starts[0].wait()
    starts[1].wait()
    pl.semaphore_wait(barrier, len(peers))

    sends = []

    def region(first, count, p, at, core, half):
        pick = lambda v: slice(None) if v is None else v
        rows = slice(None) if half is None else pl.ds(16 * half, 16)
        lanes = slice(None) if at["x"] is None else cols(at["x"], 128)
        return W.at[pl.ds(first, count), p, pick(at["z"]), pick(at["y"]), core, rows, lanes]

    def held(p, phase, coordinate):
        at = dict(me)
        for d in ORDERS[p][:phase]:
            at[d] = None
        at[ORDERS[p][phase]] = coordinate
        return at

    def remote(src, dst, ssem, rsem, to):
        return pltpu.make_async_remote_copy(
            src_ref=src, dst_ref=dst, send_sem=ssem, recv_sem=rsem, device_id=to, device_id_type=MESH
        )

    def ring(p, phase, first, count, ssem, rsem):
        d = ORDERS[p][phase]
        mine = me[d]

        def copy(kind):
            step = 1 if kind in (0, 2) else -1
            half = None if kind < 2 else kind - 2
            origin = mine if kind < 2 else wrap(mine - step, 4)
            part = region(first, count, p, held(p, phase, origin), c, half)
            return remote(part, part, ssem.at[kind], rsem.at[kind], device(d, step))

        def arrived(kind):
            step = 1 if kind in (0, 2) else -1
            half = None if kind < 2 else kind - 2
            origin = wrap(mine - step * (1 if kind < 2 else 2), 4)
            part = region(first, count, p, held(p, phase, origin), c, half)
            remote(part, part, ssem.at[kind], rsem.at[kind], device(d, step)).wait_recv()

        return copy, arrived

    def go(copy):
        copy.start()
        sends.append(copy)

    rings1 = [ring(p, 0, 0, LAYERS, s1.at[p], r1.at[p]) for p in range(3)]
    rings2 = [[ring(p, 1, f, n, s2.at[g, p], r2.at[g, p]) for p in range(3)] for g, (f, n) in enumerate(GROUPS)]
    rings3 = [[ring(p, 2, l, 1, s3.at[l, p], r3.at[l, p]) for p in range(3)] for l in range(LAYERS)]

    def send_full(rings):
        for kind in (0, 1):
            for copy, _ in rings:
                go(copy(kind))

    def forward(rings):
        for kind in (0, 1):
            for copy, arrived in rings:
                arrived(kind)
                go(copy(kind + 2))

    def finish(rings):
        for kind in (2, 3):
            for _, arrived in rings:
                arrived(kind)

    for kind in (0, 1):
        for p in (0, 1):
            go(rings1[p][0](kind))
    place.wait()
    for kind in (0, 1):
        go(rings1[2][0](kind))
    for k, to in enumerate(x_peers):
        go(remote(tok.at[to[1]], X.at[pl.ds(64, 64), cols(x, 256)], st.at[k], rt.at[k], to))
    forward(rings1)
    for k, to in enumerate(x_peers):
        go(remote(taps, T.at[x], sp_.at[k, 0], rp_.at[k, 0], to))
        go(remote(bias, S.at[x, 0], sp_.at[k, 1], rp_.at[k, 1], to))
        go(remote(lng, S.at[x, 1], sp_.at[k, 2], rp_.at[k, 2], to))
        go(remote(lnb, S.at[x, 2], sp_.at[k, 3], rp_.at[k, 3], to))
    finish(rings1)

    send_full(rings2[0])
    starts[3].wait()
    for k in range(3):
        origin = wrap(x - (k + 1), 4)
        part = X.at[pl.ds(64, 64), cols(origin, 256)]
        remote(part, part, st.at[k], rt.at[k], x_peers[k]).wait_recv()
    core_rows = X.at[pl.ds(64, 64)]
    go(remote(core_rows, X.at[pl.ds(0, 64)], sh.at[0], rh.at[0], right))
    go(remote(core_rows, X.at[pl.ds(128, 64)], sh.at[1], rh.at[1], left))
    send_full(rings2[1])
    forward(rings2[0])

    def hand(l, p, kind):
        step, half = ((0, None), (1, None), (-1, None), (2, 0), (2, 1))[kind]
        at = held(p, 2, wrap(me[ORDERS[p][2]] - step, 4))
        part = region(l, 1, p, at, c, half)
        go(remote(part, part, sd.at[l, p, kind], rd.at[l, p, kind], partner))

    def handed(l):
        for kind, (step, half) in enumerate(((0, None), (1, None), (-1, None), (2, 0), (2, 1))):
            for p in range(3):
                at = held(p, 2, wrap(me[ORDERS[p][2]] - step, 4))
                part = region(l, 1, p, at, 1 - c, half)
                remote(part, part, sd.at[l, p, kind], rd.at[l, p, kind], partner).wait_recv()

    def full3(l):
        send_full(rings3[l])
        for p in range(3):
            hand(l, p, 0)

    def forward3(l):
        for kind in (0, 1):
            for p, (copy, arrived) in enumerate(rings3[l]):
                arrived(kind)
                go(copy(kind + 2))
                hand(l, p, kind + 1)

    def finish3(l):
        for kind in (2, 3):
            for p, (_, arrived) in enumerate(rings3[l]):
                arrived(kind)
                hand(l, p, kind + 1)

    finish(rings2[0])
    full3(0)
    forward(rings2[1])
    finish(rings2[1])
    full3(1)
    forward3(0)
    full3(2)

    for k in range(4, 9):
        starts[k].wait()
    for k in range(3):
        origin = wrap(x - (k + 1), 4)
        for j, part in enumerate((T.at[origin], S.at[origin, 0], S.at[origin, 1], S.at[origin, 2])):
            remote(part, part, sp_.at[k, j], rp_.at[k, j], x_peers[k]).wait_recv()
    for k, rows in enumerate((0, 128)):
        part = X.at[pl.ds(rows, 64)]
        remote(core_rows, part, sh.at[k], rh.at[k], (right, left)[k]).wait_recv()

    def norm(l):
        low, rows = STEP * l, 192 - 2 * STEP * l
        src = X if l == 0 else Y
        g = gainv[l : l + 1, :]

        @pl.loop(0, rows // 16)
        def _(i):
            r = pl.multiple_of(low + i * 16, 16)
            v = src[pl.ds(r, 16), :].astype(F32)
            scaled = v * lax.rsqrt(jnp.mean(v * v, axis=-1, keepdims=True) + EPSILON)
            N[pl.ds(r, 16), :] = (scaled * g).astype(BF16)

    def project(l, p, dst):
        low, rows = STEP * l, 192 - 2 * STEP * l
        w = W[l, p].reshape(1024, 512)
        dst[pl.ds(low, rows), :] = jnp.dot(N[pl.ds(low, rows), :], w, preferred_element_type=F32)

    def gating(l):
        low, rows = STEP * l, 192 - 2 * STEP * l

        @pl.loop(0, rows // 16)
        def _(i):
            r = pl.multiple_of(low + i * 16, 16)
            at = pl.ds(r, 16)
            g = (V[at, :] * jax.nn.sigmoid(G[at, :])).astype(BF16).astype(F32)
            where = sp * 64 - 64 + r + lax.broadcasted_iota(jnp.int32, (16, 512), 0)
            g = jnp.where((where >= 0) & (where < 2048), g, 0.0)
            for j in range(4):
                GT[j, at, :] = g[:, 128 * j : 128 * j + 128]

    def conv(l):
        low, rows = STEP * (l + 1), 192 - 2 * STEP * (l + 1)
        for j in range(4):
            for r in range(low, low + rows, CHUNK):
                acc = jnp.zeros((CHUNK, 128), F32) + S[j, 0, l : l + 1, :]
                for k in range(TAPS):
                    acc = acc + GT[j, r + k - 15 : r + k - 15 + CHUNK, :] * T[j, l, k : k + 1, :]
                CV[r : r + CHUNK, 128 * j : 128 * j + 128] = acc

    def channel_norm(l):
        low, rows = STEP * (l + 1), 192 - 2 * STEP * (l + 1)
        g = jnp.concatenate([S[j, 1, l : l + 1, :] for j in range(4)], axis=1)
        b = jnp.concatenate([S[j, 2, l : l + 1, :] for j in range(4)], axis=1)

        @pl.loop(0, rows // 16)
        def _(i):
            at = pl.ds(pl.multiple_of(low + i * 16, 16), 16)
            v = CV[at, :]
            centered = v - jnp.mean(v, axis=-1, keepdims=True)
            spread = jnp.mean(centered * centered, axis=-1, keepdims=True)
            v = centered * lax.rsqrt(spread + EPSILON) * g + b
            A[at, :] = (v * jax.nn.sigmoid(v)).astype(BF16)

    def output(l):
        low, rows = STEP * (l + 1), 192 - 2 * STEP * (l + 1)
        src = X if l == 0 else Y
        for q in range(4):
            w = W[l, 2, q].reshape(256, 512)
            branch = lax.dot_general(
                A[pl.ds(low, rows), :], w, (((1,), (1,)), ((), ())), preferred_element_type=F32
            )
            lanes = slice(256 * q, 256 * q + 256)
            total = (src[low : low + rows, lanes].astype(F32) + branch).astype(BF16)
            if l + 1 < LAYERS:
                Y[low : low + rows, lanes] = total
            else:
                O[q] = total

    def compute(l, between=()):
        steps = [
            functools.partial(norm, l),
            functools.partial(project, l, 0, V),
            functools.partial(project, l, 1, G),
            functools.partial(gating, l),
            functools.partial(conv, l),
            functools.partial(channel_norm, l),
            functools.partial(output, l),
        ]
        between = dict(between)
        for i, step in enumerate(steps):
            if i in between:
                between[i]()
            step()

    forward3(1)
    finish3(0)
    full3(3)
    handed(0)
    compute(0, {3: lambda: forward3(2), 5: lambda: finish3(1)})
    handed(1)
    compute(1, {3: lambda: forward3(3), 5: lambda: finish3(2)})
    handed(2)
    compute(2, {5: lambda: finish3(3)})
    handed(3)
    compute(3)

    mine = pltpu.make_async_copy(O.at[x], out.at[x], loc.at[10])
    mine.start()
    for k, to in enumerate(x_peers):
        go(remote(O.at[to[1]], out.at[x], so.at[k], ro.at[k], to))
    for k in range(3):
        part = out.at[wrap(x - (k + 1), 4)]
        remote(O.at[0], part, so.at[k], ro.at[k], x_peers[k]).wait_recv()
    mine.wait()
    for copy in sends:
        copy.wait_send()


def shards(tokens, norm_gain, val_weight, gate_weight, conv_taps, conv_bias, ln_gain, ln_shift, out_weight):
    any_ = pl.BlockSpec(memory_space=pl.ANY)
    dma = pltpu.SemaphoreType.DMA
    vmem = pltpu.VMEM
    return pl.pallas_call(
        kernel,
        name="conv_stack",
        out_shape=jax.ShapeDtypeStruct(tokens.shape, tokens.dtype),
        in_specs=[any_] * 9,
        out_specs=any_,
        scratch_shapes=[
            vmem((LAYERS, 3, 4, 4, 2, 32, 512), BF16),
            vmem((LAYERS, 128, 32), BF16),
            vmem((LAYERS, 32, 128), BF16),
            vmem((192, 1024), BF16),
            vmem((192, 1024), BF16),
            vmem((192, 1024), BF16),
            vmem((192, 512), F32),
            vmem((192, 512), F32),
            vmem((4, 192, 128), F32),
            vmem((192, 512), F32),
            vmem((192, 512), BF16),
            vmem((4, 64, 256), BF16),
            vmem((LAYERS, 1024), F32),
            vmem((4, LAYERS, TAPS, 128), F32),
            vmem((4, 3, LAYERS, 128), F32),
            dma((11,)),
            dma((3, 4)), dma((3, 4)),
            dma((2, 3, 4)), dma((2, 3, 4)),
            dma((LAYERS, 3, 4)), dma((LAYERS, 3, 4)),
            dma((LAYERS, 3, 5)), dma((LAYERS, 3, 5)),
            dma((3,)), dma((3,)),
            dma((2,)), dma((2,)),
            dma((3, 4)), dma((3, 4)),
            dma((3,)), dma((3,)),
        ],
        compiler_params=pltpu.CompilerParams(
            collective_id=0, has_side_effects=True, vmem_limit_bytes=40 * 1024 * 1024
        ),
    )(tokens, norm_gain, val_weight, gate_weight, conv_taps, conv_bias, ln_gain, ln_shift, out_weight)


def solution(mesh):
    return jax.shard_map(
        shards,
        mesh=mesh,
        in_specs=(
            P(None, "sp", "tp"),
            P(),
            P(None, "sp", "tp"),
            P(None, "sp", "tp"),
            P(None, None, "tp"),
            P(None, "tp"),
            P(None, "tp"),
            P(None, "tp"),
            P(None, "tp", "sp"),
        ),
        out_specs=P(None, "sp", "tp"),
        check_vma=False,
    )
```

time: 336 us -> 63.3 us (0.19)
  waiting for transfers between devices: 267 us -> 0 us
  Pallas kernels: 0 us -> 60.7 us
  blocking collectives: 21.3 us -> 0 us
  between operations: 13.8 us -> 0.07 us
  matrix products: 10.7 us -> 0 us
  starting transfers between devices: 7.9 us -> 0 us
  other arithmetic: 7.6 us -> 0 us
  local copies, waits for them, and re-layouts: 5.73 us -> 2.28 us
    all_gather x6 -> x0, waiting for transfers between devices: 262 us -> none  [the longest x3 136 us: whole(): w = lax.all_gather(w, 'sp', axis=dim, tiled=True)]
    pallas_call x0 -> x1, Pallas kernels: none -> 60.7 us  [shards(): pl.pallas_call(kernel, name='conv_stack', out_shape=jax.ShapeDtypeStruct(...]
    all_gather x1 -> x0, blocking collectives: 13 us -> none  [shards(): lax.all_gather(jnp.concatenate([conv_taps, conv_bias[:, None], ln_gain[:,...]
    dot_general x12 -> x0, matrix products: 10.7 us -> none  [the longest x4 4.18 us: shards(): gate = jnp.dot(normed, gates[layer], preferred_element_type=jnp.float32)]
    all_to_all x1 -> x0, blocking collectives: 8.3 us -> none  [shards(): return lax.all_to_all(stream[None], 'tp', 2, 0, tiled=True)]
    reduce_sum x9 -> x0, other arithmetic: 4.27 us -> none  [the longest x4 3.37 us: shards(): mean = jnp.mean(convolved, axis=-1, keepdims=True)]
    all_to_all x1 -> x0, starting transfers between devices: 3.98 us -> none  [shards(): own = lax.all_to_all(tokens, 'tp', 0, 2, tiled=True)[0]]
    ppermute x2 -> x0, starting transfers between devices: 3.73 us -> none  [the longest x1 2.97 us: shards(): after = lax.ppermute(own, 'sp', down)]
  transfers between devices with their start and end apart: 9 -> 0, of which waited for: 7 -> 0; matrix products, arithmetic and copies ran while one was open for 2% -> 0% of each run, Pallas kernels for 0% -> 0%
where the time goes in v2:
time: 63.3 us; the launch traced here: 63.1 us
  Pallas kernels  60.7 us (96%)
  local copies, waits for them, and re-layouts  2.28 us (4%)
    pallas_call x1, Pallas kernels, shards(): pl.pallas_call(kernel, name='conv_stack', out_shape=jax.ShapeDtypeStruct(...  60.7 us
    unnamed x19, local copies, waits for them, and re-layouts  2.28 us

profile of v2, /device:TPU:1, one launch (start us, length us, event | category | flops | bytes accessed | tf_op | source)
XLA Modules:
  0.0 63.1 jit_solution(16946574535240984708)
XLA Ops:
  0.0 0.0 copy-start.7
  0.0 0.0 copy-start
  0.0 0.9 %copy.10.taps = f32[4,31,128]{2,1,0:T(8,128)S(1)} copy(f32[4,31,128]{2,0,1:T(4,128)} %param.13) | data formatting | bytes 126976 | tf_op args[4]
  0.9 0.0 copy-done.7
  0.9 0.0 copy-start.1
  0.9 0.0 copy-start.2
  0.9 0.0 copy-start.3
  0.9 0.0 copy-start.4
  0.9 0.0 copy-start.5
  0.9 0.0 copy-start.6
  1.0 0.1 copy.11.outw
  1.1 0.0 copy-done
  1.1 0.6 copy-done.1
  1.7 0.0 copy-done.2
  1.7 0.0 copy-done.3
  1.7 0.0 copy-done.4
  1.7 0.0 copy-done.5
  1.7 0.0 copy-done.6
  1.7 60.7 %conv_stack.1 = bf16[4,64,256]{2,1,0:T(8,128)(2,1)S(1)} custom-call(bf16[4,64,256]{2,1,0:T(8,128)(2,1)S(1)} %copy-done, f32[4,1024]{1,0:T(4,128)S(1)} %copy-done.3, bf16[4,32,128]{2,1,0:T(8,128)(2,1)S(1)} %copy-done.1, bf16[4,32,128]{2,1,0:T(8,128)(2,1)S(1)} %copy-done.2, f32[4,31,128]{2,1,0:T(8,128)S(1)} %copy.10.taps, f32[4,128]{1,0:T(4,128)S(1)} %copy-done.4, ...), custom_call_target="tpu_custom_call" | custom-call | tf_op jit(solution)/shard_map/conv_stack/pallas_call | solution.py:335
  62.4 0.7 %copy.13 = bf16[4,64,256]{2,1,0:T(8,128)(2,1)} copy(bf16[4,64,256]{2,1,0:T(8,128)(2,1)S(1)} %conv_stack.1) | data formatting | bytes 262144
Async XLA Ops:
  0.0 0.9 %copy-start.7 = (bf16[4,128,32]{1,2,0:T(8,128)(2,1)S(1)}, bf16[4,128,32]{1,2,0:T(8,128)(2,1)}, u32[]{:S(2)}) copy-start(bf16[4,128,32]{1,2,0:T(8,128)(2,1)} %param.17) | copy-start | bytes 98308
  0.0 1.1 %copy-start = (bf16[4,64,256]{2,1,0:T(8,128)(2,1)S(1)}, bf16[4,64,256]{2,1,0:T(8,128)(2,1)}, u32[]{:S(2)}) copy-start(bf16[4,64,256]{2,1,0:T(8,128)(2,1)} %tok.1) | copy-start | bytes 393220
  0.9 0.8 %copy-start.1 = (bf16[4,32,128]{2,1,0:T(8,128)(2,1)S(1)}, bf16[4,32,128]{2,1,0:T(8,128)(2,1)}, u32[]{:S(2)}) copy-start(bf16[4,32,128]{2,1,0:T(8,128)(2,1)} %val.1) | copy-start | bytes 98308
  0.9 0.8 %copy-start.2 = (bf16[4,32,128]{2,1,0:T(8,128)(2,1)S(1)}, bf16[4,32,128]{2,1,0:T(8,128)(2,1)}, u32[]{:S(2)}) copy-start(bf16[4,32,128]{2,1,0:T(8,128)(2,1)} %gate.1) | copy-start | bytes 98308
  0.9 0.8 %copy-start.3 = (f32[4,1024]{1,0:T(4,128)S(1)}, f32[4,1024]{1,0:T(4,128)}, u32[]{:S(2)}) copy-start(f32[4,1024]{1,0:T(4,128)} %gain.1) | copy-start | bytes 49156
  0.9 0.8 %copy-start.4 = (f32[4,128]{1,0:T(4,128)S(1)}, f32[4,128]{1,0:T(4,128)}, u32[]{:S(2)}) copy-start(f32[4,128]{1,0:T(4,128)} %bias.1) | copy-start | bytes 6148
  0.9 0.8 %copy-start.5 = (f32[4,128]{1,0:T(4,128)S(1)}, f32[4,128]{1,0:T(4,128)}, u32[]{:S(2)}) copy-start(f32[4,128]{1,0:T(4,128)} %lng.1) | copy-start | bytes 6148
  0.9 0.7 %copy-start.6 = (f32[4,128]{1,0:T(4,128)S(1)}, f32[4,128]{1,0:T(4,128)}, u32[]{:S(2)}) copy-start(f32[4,128]{1,0:T(4,128)} %lnb.1) | copy-start | bytes 6148

commit v3 on v2

--- a/solution.py
+++ b/solution.py
@@ -24,7 +24,7 @@
 
 def kernel(
     tok, gain, val, gate, taps, bias, lng, lnb, outw, out,
-    W, ow, ost, X, Y, N, V, G, GT, CV, A, O, gainv, T, S,
+    W, X, Y, N, V, G, GT, CV, A, O, gainv, T,
     loc, s1, r1, s2, r2, s3, r3, sd, rd, st, rt, sh, rh, sp_, rp_, so, ro,
 ):
     sp = lax.axis_index("sp")
@@ -41,42 +41,29 @@
         return ((at["z"] * 4 + at["y"]) * 2 + c, at["x"])
 
     partner = (sp + 1 - 2 * c, x)
-    left, right = (wrap(sp - 1, n_sp), x), (wrap(sp + 1, n_sp), x)
     across = (wrap(sp + 1 - 2 * (1 - c), n_sp), x)
     x_peers = [(sp, wrap(x + k, 4)) for k in (1, 2, 3)]
 
+    barrier = pltpu.get_barrier_semaphore()
+    peers = [device(d, step) for d in "xyz" for step in (1, -1)] + [partner]
+    for peer in peers:
+        pl.semaphore_signal(barrier, inc=1, device_id=peer, device_id_type=MESH)
+
     cols = lambda i, w: pl.ds(pl.multiple_of(i * w, w), w)
-    starts = [
-        pltpu.make_async_copy(val, W.at[:, 0, z, y, c, :, cols(x, 128)], loc.at[0]),
-        pltpu.make_async_copy(gate, W.at[:, 1, z, y, c, :, cols(x, 128)], loc.at[1]),
-        pltpu.make_async_copy(outw, ow, loc.at[2]),
+    parts = (val, gate, outw)
+    starts = [pltpu.make_async_copy(w, W.at[:, p, z, y, c, :, cols(x, 128)], loc.at[p]) for p, w in enumerate(parts)]
+    starts += [
         pltpu.make_async_copy(tok.at[x], X.at[pl.ds(64, 64), cols(x, 256)], loc.at[3]),
         pltpu.make_async_copy(gain, gainv, loc.at[4]),
-        pltpu.make_async_copy(taps, T.at[x], loc.at[5]),
-        pltpu.make_async_copy(bias, S.at[x, 0], loc.at[6]),
-        pltpu.make_async_copy(lng, S.at[x, 1], loc.at[7]),
-        pltpu.make_async_copy(lnb, S.at[x, 2], loc.at[8]),
+        pltpu.make_async_copy(taps, T.at[x, pl.ds(0, TAPS)], loc.at[5]),
+        pltpu.make_async_copy(bias, T.at[x, TAPS], loc.at[6]),
+        pltpu.make_async_copy(lng, T.at[x, TAPS + 1], loc.at[7]),
+        pltpu.make_async_copy(lnb, T.at[x, TAPS + 2], loc.at[8]),
     ]
     for copy in starts:
         copy.start()
-
-    barrier = pltpu.get_barrier_semaphore()
-    peers = x_peers + [device("y", 1), device("y", -1), device("z", 1), device("z", -1), partner, across]
-    for peer in peers:
-        pl.semaphore_signal(barrier, inc=1, device_id=peer, device_id_type=MESH)
-
-    starts[2].wait()
-    eye = (
-        lax.broadcasted_iota(jnp.int32, (32, 32), 0) == lax.broadcasted_iota(jnp.int32, (32, 32), 1)
-    ).astype(BF16)
-    for l in range(LAYERS):
-        ost[l] = lax.dot_general(
-            eye, ow[l], (((1,), (1,)), ((), ())), preferred_element_type=F32
-        ).astype(BF16)
-    place = pltpu.make_async_copy(ost, W.at[:, 2, z, y, c, :, cols(x, 128)], loc.at[9])
-    place.start()
-    starts[0].wait()
-    starts[1].wait()
+    for copy in starts:
+        copy.wait()
     pl.semaphore_wait(barrier, len(peers))
 
     sends = []
@@ -143,33 +130,35 @@
             for _, arrived in rings:
                 arrived(kind)
 
-    for kind in (0, 1):
-        for p in (0, 1):
-            go(rings1[p][0](kind))
-    place.wait()
-    for kind in (0, 1):
-        go(rings1[2][0](kind))
-    for k, to in enumerate(x_peers):
-        go(remote(tok.at[to[1]], X.at[pl.ds(64, 64), cols(x, 256)], st.at[k], rt.at[k], to))
+    send_full(rings1)
+
+    def send_tokens(k):
+        go(remote(tok.at[x_peers[k][1]], X.at[pl.ds(64, 64), cols(x, 256)], st.at[k], rt.at[k], x_peers[k]))
+
+    share = pl.ds(17 * c, 17)
+
+    def send_parameters(k):
+        go(remote(T.at[x, share], T.at[x, share], sp_.at[0, k], rp_.at[0, k], x_peers[k]))
+
+    for k in (0, 2):
+        send_tokens(k)
+    for k in (0, 2):
+        send_parameters(k)
     forward(rings1)
-    for k, to in enumerate(x_peers):
-        go(remote(taps, T.at[x], sp_.at[k, 0], rp_.at[k, 0], to))
-        go(remote(bias, S.at[x, 0], sp_.at[k, 1], rp_.at[k, 1], to))
-        go(remote(lng, S.at[x, 1], sp_.at[k, 2], rp_.at[k, 2], to))
-        go(remote(lnb, S.at[x, 2], sp_.at[k, 3], rp_.at[k, 3], to))
     finish(rings1)
 
     send_full(rings2[0])
-    starts[3].wait()
+    send_tokens(1)
+    send_parameters(1)
+    send_full(rings2[1])
+    forward(rings2[0])
     for k in range(3):
-        origin = wrap(x - (k + 1), 4)
-        part = X.at[pl.ds(64, 64), cols(origin, 256)]
+        part = X.at[pl.ds(64, 64), cols(wrap(x - (k + 1), 4), 256)]
         remote(part, part, st.at[k], rt.at[k], x_peers[k]).wait_recv()
     core_rows = X.at[pl.ds(64, 64)]
-    go(remote(core_rows, X.at[pl.ds(0, 64)], sh.at[0], rh.at[0], right))
-    go(remote(core_rows, X.at[pl.ds(128, 64)], sh.at[1], rh.at[1], left))
-    send_full(rings2[1])
-    forward(rings2[0])
+    near = X.at[pl.ds(128 * c, 64)]
+    far = X.at[pl.ds(128 - 128 * c, 64)]
+    go(remote(core_rows, near, sh.at[0], rh.at[0], partner))
 
     def hand(l, p, kind):
         step, half = ((0, None), (1, None), (-1, None), (2, 0), (2, 1))[kind]
@@ -177,8 +166,9 @@
         part = region(l, 1, p, at, c, half)
         go(remote(part, part, sd.at[l, p, kind], rd.at[l, p, kind], partner))
 
-    def handed(l):
-        for kind, (step, half) in enumerate(((0, None), (1, None), (-1, None), (2, 0), (2, 1))):
+    def handed(l, kinds=(0, 1, 2, 3, 4)):
+        for kind in kinds:
+            step, half = ((0, None), (1, None), (-1, None), (2, 0), (2, 1))[kind]
             for p in range(3):
                 at = held(p, 2, wrap(me[ORDERS[p][2]] - step, 4))
                 part = region(l, 1, p, at, 1 - c, half)
@@ -204,21 +194,19 @@
 
     finish(rings2[0])
     full3(0)
+    handed(0, (0,))
+    go(remote(core_rows, far, sh.at[1], rh.at[1], across))
     forward(rings2[1])
     finish(rings2[1])
     full3(1)
     forward3(0)
     full3(2)
 
-    for k in range(4, 9):
-        starts[k].wait()
     for k in range(3):
         origin = wrap(x - (k + 1), 4)
-        for j, part in enumerate((T.at[origin], S.at[origin, 0], S.at[origin, 1], S.at[origin, 2])):
-            remote(part, part, sp_.at[k, j], rp_.at[k, j], x_peers[k]).wait_recv()
-    for k, rows in enumerate((0, 128)):
-        part = X.at[pl.ds(rows, 64)]
-        remote(core_rows, part, sh.at[k], rh.at[k], (right, left)[k]).wait_recv()
+        part = T.at[origin, share]
+        remote(part, part, sp_.at[0, k], rp_.at[0, k], x_peers[k]).wait_recv()
+        go(remote(part, part, sp_.at[1, k], rp_.at[1, k], partner))
 
     def norm(l):
         low, rows = STEP * l, 192 - 2 * STEP * l
@@ -254,15 +242,15 @@
         low, rows = STEP * (l + 1), 192 - 2 * STEP * (l + 1)
         for j in range(4):
             for r in range(low, low + rows, CHUNK):
-                acc = jnp.zeros((CHUNK, 128), F32) + S[j, 0, l : l + 1, :]
+                acc = jnp.zeros((CHUNK, 128), F32) + T[j, TAPS, l : l + 1, :]
                 for k in range(TAPS):
-                    acc = acc + GT[j, r + k - 15 : r + k - 15 + CHUNK, :] * T[j, l, k : k + 1, :]
+                    acc = acc + GT[j, r + k - 15 : r + k - 15 + CHUNK, :] * T[j, k, l : l + 1, :]
                 CV[r : r + CHUNK, 128 * j : 128 * j + 128] = acc
 
     def channel_norm(l):
         low, rows = STEP * (l + 1), 192 - 2 * STEP * (l + 1)
-        g = jnp.concatenate([S[j, 1, l : l + 1, :] for j in range(4)], axis=1)
-        b = jnp.concatenate([S[j, 2, l : l + 1, :] for j in range(4)], axis=1)
+        g = jnp.concatenate([T[j, TAPS + 1, l : l + 1, :] for j in range(4)], axis=1)
+        b = jnp.concatenate([T[j, TAPS + 2, l : l + 1, :] for j in range(4)], axis=1)
 
         @pl.loop(0, rows // 16)
         def _(i):
@@ -307,7 +295,13 @@
     forward3(1)
     finish3(0)
     full3(3)
-    handed(0)
+    handed(0, (1, 2, 3, 4))
+    for k in range(3):
+        origin = wrap(x - (k + 1), 4)
+        part = T.at[origin, pl.ds(17 - 17 * c, 17)]
+        remote(part, part, sp_.at[1, k], rp_.at[1, k], partner).wait_recv()
+    remote(core_rows, far, sh.at[0], rh.at[0], partner).wait_recv()
+    remote(core_rows, near, sh.at[1], rh.at[1], across).wait_recv()
     compute(0, {3: lambda: forward3(2), 5: lambda: finish3(1)})
     handed(1)
     compute(1, {3: lambda: forward3(3), 5: lambda: finish3(2)})
@@ -340,8 +334,6 @@
         out_specs=any_,
         scratch_shapes=[
             vmem((LAYERS, 3, 4, 4, 2, 32, 512), BF16),
-            vmem((LAYERS, 128, 32), BF16),
-            vmem((LAYERS, 32, 128), BF16),
             vmem((192, 1024), BF16),
             vmem((192, 1024), BF16),
             vmem((192, 1024), BF16),
@@ -352,8 +344,7 @@
             vmem((192, 512), BF16),
             vmem((4, 64, 256), BF16),
             vmem((LAYERS, 1024), F32),
-            vmem((4, LAYERS, TAPS, 128), F32),
-            vmem((4, 3, LAYERS, 128), F32),
+            vmem((4, TAPS + 3, LAYERS, 128), F32),
             dma((11,)),
             dma((3, 4)), dma((3, 4)),
             dma((2, 3, 4)), dma((2, 3, 4)),
@@ -361,13 +352,16 @@
             dma((LAYERS, 3, 5)), dma((LAYERS, 3, 5)),
             dma((3,)), dma((3,)),
             dma((2,)), dma((2,)),
-            dma((3, 4)), dma((3, 4)),
+            dma((2, 3)), dma((2, 3)),
             dma((3,)), dma((3,)),
         ],
         compiler_params=pltpu.CompilerParams(
             collective_id=0, has_side_effects=True, vmem_limit_bytes=40 * 1024 * 1024
         ),
-    )(tokens, norm_gain, val_weight, gate_weight, conv_taps, conv_bias, ln_gain, ln_shift, out_weight)
+    )(
+        tokens, norm_gain, val_weight, gate_weight, conv_taps.transpose(1, 0, 2), conv_bias, ln_gain, ln_shift,
+        out_weight.transpose(0, 2, 1),
+    )
 
 
 def solution(mesh):

time: 63.3 us -> 68.5 us (1.082)
  local copies, waits for them, and re-layouts: 2.28 us -> 7.43 us
    unnamed x19, local copies, waits for them, and re-layouts: 2.28 us -> 7.43 us
where the time goes in v3:
time: 68.5 us; the launch traced here: 68 us
  Pallas kernels  60.5 us (88%)
  local copies, waits for them, and re-layouts  7.43 us (11%)
    pallas_call x1, Pallas kernels, shards(): pl.pallas_call(kernel, name='conv_stack', out_shape=jax.ShapeDtypeStruct(...  60.5 us
    unnamed x19, local copies, waits for them, and re-layouts  7.43 us

profile of v3, /device:TPU:1, one launch (start us, length us, event | category | flops | bytes accessed | tf_op | source)
XLA Modules:
  0.0 68.0 jit_solution(2701998072181164509)
XLA Ops:
  0.0 0.0 copy-start.6
  0.0 0.7 copy-done.6
  0.7 0.0 copy-start
  0.7 0.9 %copy-done = bf16[4,64,256]{2,1,0:T(8,128)(2,1)S(1)} copy-done((bf16[4,64,256]{2,1,0:T(8,128)(2,1)S(1)}, bf16[4,64,256]{2,1,0:T(8,128)(2,1)}, u32[]{:S(2)}) %copy-start) | copy-done | bytes 131096
  1.6 0.0 copy-start.1
  1.6 0.8 %copy-done.1 = f32[4,31,128]{2,0,1:T(4,128)S(1)} copy-done((f32[4,31,128]{2,0,1:T(4,128)S(1)}, f32[4,31,128]{2,0,1:T(4,128)}, u32[]{:S(2)}) %copy-start.1) | copy-done | bytes 63512
  2.4 0.0 copy-start.2
  2.4 0.8 %copy-done.2 = bf16[4,32,128]{2,1,0:T(8,128)(2,1)S(1)} copy-done((bf16[4,32,128]{2,1,0:T(8,128)(2,1)S(1)}, bf16[4,32,128]{2,1,0:T(8,128)(2,1)}, u32[]{:S(2)}) %copy-start.2) | copy-done | bytes 32792
  3.2 0.0 copy-start.3
  3.2 0.8 %copy-done.3 = bf16[4,32,128]{2,1,0:T(8,128)(2,1)S(1)} copy-done((bf16[4,32,128]{2,1,0:T(8,128)(2,1)S(1)}, bf16[4,32,128]{2,1,0:T(8,128)(2,1)}, u32[]{:S(2)}) %copy-start.3) | copy-done | bytes 32792
  3.9 0.0 copy-start.4
  3.9 0.8 %copy-done.4 = bf16[4,128,32]{1,2,0:T(8,128)(2,1)S(1)} copy-done((bf16[4,128,32]{1,2,0:T(8,128)(2,1)S(1)}, bf16[4,128,32]{1,2,0:T(8,128)(2,1)}, u32[]{:S(2)}) %copy-start.4) | copy-done | bytes 32792
  4.7 0.0 copy-start.5
  4.7 0.7 %copy-done.5 = f32[4,1024]{1,0:T(4,128)S(1)} copy-done((f32[4,1024]{1,0:T(4,128)S(1)}, f32[4,1024]{1,0:T(4,128)}, u32[]{:S(2)}) %copy-start.5) | copy-done | bytes 16408
  5.4 0.0 copy-start.7
  5.4 0.7 copy-done.7
  6.1 0.0 copy-start.8
  6.1 0.7 copy-done.8
  6.8 60.5 %conv_stack.1 = bf16[4,64,256]{2,1,0:T(8,128)(2,1)S(1)} custom-call(bf16[4,64,256]{2,1,0:T(8,128)(2,1)S(1)} %copy-done, f32[4,1024]{1,0:T(4,128)S(1)} %copy-done.5, bf16[4,32,128]{2,1,0:T(8,128)(2,1)S(1)} %copy-done.2, bf16[4,32,128]{2,1,0:T(8,128)(2,1)S(1)} %copy-done.3, f32[31,4,128]{2,1,0:T(4,128)S(1)} %bitcast.2, f32[4,128]{1,0:T(4,128)S(1)} %copy-done.6, ...), custom_call_target="tpu_custom_call" | custom-call | tf_op jit(solution)/shard_map/conv_stack/pallas_call | solution.py:329
  67.3 0.7 copy.11
Async XLA Ops:
  0.0 0.7 %copy-start.6 = (f32[4,128]{1,0:T(4,128)S(1)}, f32[4,128]{1,0:T(4,128)}, u32[]{:S(2)}) copy-start(f32[4,128]{1,0:T(4,128)} %bias.1) | copy-start | bytes 6148
  0.7 0.9 %copy-start = (bf16[4,64,256]{2,1,0:T(8,128)(2,1)S(1)}, bf16[4,64,256]{2,1,0:T(8,128)(2,1)}, u32[]{:S(2)}) copy-start(bf16[4,64,256]{2,1,0:T(8,128)(2,1)} %tok.1) | copy-start | bytes 393220
  1.6 0.8 %copy-start.1 = (f32[4,31,128]{2,0,1:T(4,128)S(1)}, f32[4,31,128]{2,0,1:T(4,128)}, u32[]{:S(2)}) copy-start(f32[4,31,128]{2,0,1:T(4,128)} %param.13) | copy-start | bytes 190468
  2.4 0.8 %copy-start.2 = (bf16[4,32,128]{2,1,0:T(8,128)(2,1)S(1)}, bf16[4,32,128]{2,1,0:T(8,128)(2,1)}, u32[]{:S(2)}) copy-start(bf16[4,32,128]{2,1,0:T(8,128)(2,1)} %val.1) | copy-start | bytes 98308
  3.2 0.8 %copy-start.3 = (bf16[4,32,128]{2,1,0:T(8,128)(2,1)S(1)}, bf16[4,32,128]{2,1,0:T(8,128)(2,1)}, u32[]{:S(2)}) copy-start(bf16[4,32,128]{2,1,0:T(8,128)(2,1)} %gate.1) | copy-start | bytes 98308
  3.9 0.8 %copy-start.4 = (bf16[4,128,32]{1,2,0:T(8,128)(2,1)S(1)}, bf16[4,128,32]{1,2,0:T(8,128)(2,1)}, u32[]{:S(2)}) copy-start(bf16[4,128,32]{1,2,0:T(8,128)(2,1)} %param.17) | copy-start | bytes 98308
  4.7 0.7 %copy-start.5 = (f32[4,1024]{1,0:T(4,128)S(1)}, f32[4,1024]{1,0:T(4,128)}, u32[]{:S(2)}) copy-start(f32[4,1024]{1,0:T(4,128)} %gain.1) | copy-start | bytes 49156
  5.4 0.7 %copy-start.7 = (f32[4,128]{1,0:T(4,128)S(1)}, f32[4,128]{1,0:T(4,128)}, u32[]{:S(2)}) copy-start(f32[4,128]{1,0:T(4,128)} %lng.1) | copy-start | bytes 6148
  6.1 0.7 %copy-start.8 = (f32[4,128]{1,0:T(4,128)S(1)}, f32[4,128]{1,0:T(4,128)}, u32[]{:S(2)}) copy-start(f32[4,128]{1,0:T(4,128)} %lnb.1) | copy-start | bytes 6148

commit v4 on v3

--- a/solution.py
+++ b/solution.py
@@ -45,7 +45,7 @@
     x_peers = [(sp, wrap(x + k, 4)) for k in (1, 2, 3)]
 
     barrier = pltpu.get_barrier_semaphore()
-    peers = [device(d, step) for d in "xyz" for step in (1, -1)] + [partner]
+    peers = [device(d, step) for d in "xyz" for step in (1, 2, 3)] + [partner]
     for peer in peers:
         pl.semaphore_signal(barrier, inc=1, device_id=peer, device_id_type=MESH)
 
@@ -110,28 +110,38 @@
         copy.start()
         sends.append(copy)
 
-    rings1 = [ring(p, 0, 0, LAYERS, s1.at[p], r1.at[p]) for p in range(3)]
-    rings2 = [[ring(p, 1, f, n, s2.at[g, p], r2.at[g, p]) for p in range(3)] for g, (f, n) in enumerate(GROUPS)]
+    def spread(p, phase, first, count, ssem, rsem):
+        d = ORDERS[p][phase]
+
+        def copy(k):
+            part = region(first, count, p, held(p, phase, me[d]), c, None)
+            return remote(part, part, ssem.at[k - 1], rsem.at[k - 1], device(d, k))
+
+        def arrived(k):
+            part = region(first, count, p, held(p, phase, wrap(me[d] - k, 4)), c, None)
+            remote(part, part, ssem.at[k - 1], rsem.at[k - 1], device(d, k)).wait_recv()
+
+        return copy, arrived
+
+    spreads1 = [[spread(p, 0, f, n, s1.at[g, p], r1.at[g, p]) for p in range(3)] for g, (f, n) in enumerate(GROUPS)]
+    spreads2 = [[spread(p, 1, f, n, s2.at[g, p], r2.at[g, p]) for p in range(3)] for g, (f, n) in enumerate(GROUPS)]
     rings3 = [[ring(p, 2, l, 1, s3.at[l, p], r3.at[l, p]) for p in range(3)] for l in range(LAYERS)]
+
+    def send_spread(spreads):
+        for k in (2, 1, 3):
+            for copy, _ in spreads:
+                go(copy(k))
+
+    def end_spread(spreads):
+        for k in (1, 3, 2):
+            for _, arrived in spreads:
+                arrived(k)
 
     def send_full(rings):
         for kind in (0, 1):
             for copy, _ in rings:
                 go(copy(kind))
 
-    def forward(rings):
-        for kind in (0, 1):
-            for copy, arrived in rings:
-                arrived(kind)
-                go(copy(kind + 2))
-
-    def finish(rings):
-        for kind in (2, 3):
-            for _, arrived in rings:
-                arrived(kind)
-
-    send_full(rings1)
-
     def send_tokens(k):
         go(remote(tok.at[x_peers[k][1]], X.at[pl.ds(64, 64), cols(x, 256)], st.at[k], rt.at[k], x_peers[k]))
 
@@ -140,18 +150,16 @@
     def send_parameters(k):
         go(remote(T.at[x, share], T.at[x, share], sp_.at[0, k], rp_.at[0, k], x_peers[k]))
 
-    for k in (0, 2):
+    send_spread(spreads1[0])
+    send_spread(spreads1[1])
+    for k in (1, 0, 2):
         send_tokens(k)
-    for k in (0, 2):
+    end_spread(spreads1[0])
+    send_spread(spreads2[0])
+    end_spread(spreads1[1])
+    send_spread(spreads2[1])
+    for k in (1, 0, 2):
         send_parameters(k)
-    forward(rings1)
-    finish(rings1)
-
-    send_full(rings2[0])
-    send_tokens(1)
-    send_parameters(1)
-    send_full(rings2[1])
-    forward(rings2[0])
     for k in range(3):
         part = X.at[pl.ds(64, 64), cols(wrap(x - (k + 1), 4), 256)]
         remote(part, part, st.at[k], rt.at[k], x_peers[k]).wait_recv()
@@ -192,12 +200,11 @@
                 arrived(kind)
                 hand(l, p, kind + 1)
 
-    finish(rings2[0])
+    end_spread(spreads2[0])
     full3(0)
     handed(0, (0,))
     go(remote(core_rows, far, sh.at[1], rh.at[1], across))
-    forward(rings2[1])
-    finish(rings2[1])
+    end_spread(spreads2[1])
     full3(1)
     forward3(0)
     full3(2)
@@ -323,7 +330,7 @@
 
 
 def shards(tokens, norm_gain, val_weight, gate_weight, conv_taps, conv_bias, ln_gain, ln_shift, out_weight):
-    any_ = pl.BlockSpec(memory_space=pl.ANY)
+    any_ = pl.BlockSpec(memory_space=pltpu.HBM)
     dma = pltpu.SemaphoreType.DMA
     vmem = pltpu.VMEM
     return pl.pallas_call(
@@ -331,7 +338,7 @@
         name="conv_stack",
         out_shape=jax.ShapeDtypeStruct(tokens.shape, tokens.dtype),
         in_specs=[any_] * 9,
-        out_specs=any_,
+        out_specs=pl.BlockSpec(memory_space=pl.ANY),
         scratch_shapes=[
             vmem((LAYERS, 3, 4, 4, 2, 32, 512), BF16),
             vmem((192, 1024), BF16),
@@ -346,8 +353,8 @@
             vmem((LAYERS, 1024), F32),
             vmem((4, TAPS + 3, LAYERS, 128), F32),
             dma((11,)),
-            dma((3, 4)), dma((3, 4)),
-            dma((2, 3, 4)), dma((2, 3, 4)),
+            dma((2, 3, 3)), dma((2, 3, 3)),
+            dma((2, 3, 3)), dma((2, 3, 3)),
             dma((LAYERS, 3, 4)), dma((LAYERS, 3, 4)),
             dma((LAYERS, 3, 5)), dma((LAYERS, 3, 5)),
             dma((3,)), dma((3,)),
@@ -356,7 +363,7 @@
             dma((3,)), dma((3,)),
         ],
         compiler_params=pltpu.CompilerParams(
-            collective_id=0, has_side_effects=True, vmem_limit_bytes=40 * 1024 * 1024
+            collective_id=0, has_side_effects=True, vmem_limit_bytes=67043328
         ),
     )(
         tokens, norm_gain, val_weight, gate_weight, conv_taps.transpose(1, 0, 2), conv_bias, ln_gain, ln_shift,

time: 68.5 us -> 54.3 us (0.79)
  Pallas kernels: 60.5 us -> 52.6 us
  local copies, waits for them, and re-layouts: 7.43 us -> 1.57 us
    pallas_call x1, Pallas kernels: 60.5 us -> 52.6 us  [shards(): pl.pallas_call(kernel, name='conv_stack', out_shape=jax.ShapeDtypeStruct(...]
    unnamed x19 -> x1, local copies, waits for them, and re-layouts: 7.43 us -> 1.57 us
where the time goes in v4:
time: 54.3 us; the launch traced here: 54.2 us
  Pallas kernels  52.6 us (97%)
  local copies, waits for them, and re-layouts  1.57 us (3%)
    pallas_call x1, Pallas kernels, shards(): pl.pallas_call(kernel, name='conv_stack', out_shape=jax.ShapeDtypeStruct(...  52.6 us
    unnamed x1, local copies, waits for them, and re-layouts  1.57 us

profile of v4, /device:TPU:1, one launch (start us, length us, event | category | flops | bytes accessed | tf_op | source)
XLA Modules:
  0.0 54.2 jit_solution(4846413116835270443)
XLA Ops:
  0.0 52.6 %conv_stack.1 = bf16[4,64,256]{2,1,0:T(8,128)(2,1)} custom-call(bf16[4,64,256]{2,1,0:T(8,128)(2,1)} %tok.1, f32[4,1024]{1,0:T(4,128)} %gain.1, bf16[4,32,128]{2,1,0:T(8,128)(2,1)} %val.1, bf16[4,32,128]{2,1,0:T(8,128)(2,1)} %gate.1, f32[31,4,128]{2,1,0:T(4,128)} %bitcast.2, f32[4,128]{1,0:T(4,128)} %bias.1, f32[4,128]{1,0:T(4,128)} %lng.1, f32[4,128]{1,0:T(4,128)} %lnb.1, ...), custom_call_target="tpu_custom_call" | custom-call | tf_op jit(solution)/shard_map/conv_stack/pallas_call | solution.py:336
  52.6 1.6 %copy.11 = bf16[4,64,256]{2,1,0:T(8,128)(2,1)} copy(bf16[4,64,256]{2,1,0:T(8,128)(2,1)} %conv_stack.1) | data formatting | bytes 262144

commit v5 on v4

--- a/solution.py
+++ b/solution.py
@@ -14,8 +14,10 @@
 MESH = pl.DeviceIdType.MESH
 F32, BF16 = jnp.float32, jnp.bfloat16
 ORDERS = (("x", "y", "z"), ("y", "z", "x"), ("z", "x", "y"))
-GROUPS = ((0, 1), (1, 3))
+GROUPS1 = ((0, 1), (1, 3))
+GROUPS2 = ((0, 1), (1, 1), (2, 2))
 CHUNK = 32
+NORM_CHUNK = 32
 
 
 def wrap(v, n):
@@ -89,19 +91,16 @@
     def ring(p, phase, first, count, ssem, rsem):
         d = ORDERS[p][phase]
         mine = me[d]
+        kinds = ((1, 0, 1), (-1, 1, 1), (1, 1, 1), (-1, 0, 1), (1, 0, 2), (-1, 1, 2))
 
         def copy(kind):
-            step = 1 if kind in (0, 2) else -1
-            half = None if kind < 2 else kind - 2
-            origin = mine if kind < 2 else wrap(mine - step, 4)
-            part = region(first, count, p, held(p, phase, origin), c, half)
+            step, half, hops = kinds[kind]
+            part = region(first, count, p, held(p, phase, wrap(mine - step * (hops - 1), 4)), c, half)
             return remote(part, part, ssem.at[kind], rsem.at[kind], device(d, step))
 
         def arrived(kind):
-            step = 1 if kind in (0, 2) else -1
-            half = None if kind < 2 else kind - 2
-            origin = wrap(mine - step * (1 if kind < 2 else 2), 4)
-            part = region(first, count, p, held(p, phase, origin), c, half)
+            step, half, hops = kinds[kind]
+            part = region(first, count, p, held(p, phase, wrap(mine - step * hops, 4)), c, half)
             remote(part, part, ssem.at[kind], rsem.at[kind], device(d, step)).wait_recv()
 
         return copy, arrived
@@ -123,8 +122,8 @@
 
         return copy, arrived
 
-    spreads1 = [[spread(p, 0, f, n, s1.at[g, p], r1.at[g, p]) for p in range(3)] for g, (f, n) in enumerate(GROUPS)]
-    spreads2 = [[spread(p, 1, f, n, s2.at[g, p], r2.at[g, p]) for p in range(3)] for g, (f, n) in enumerate(GROUPS)]
+    spreads1 = [[spread(p, 0, f, n, s1.at[g, p], r1.at[g, p]) for p in range(3)] for g, (f, n) in enumerate(GROUPS1)]
+    spreads2 = [[spread(p, 1, f, n, s2.at[g, p], r2.at[g, p]) for p in range(3)] for g, (f, n) in enumerate(GROUPS2)]
     rings3 = [[ring(p, 2, l, 1, s3.at[l, p], r3.at[l, p]) for p in range(3)] for l in range(LAYERS)]
 
     def send_spread(spreads):
@@ -137,11 +136,6 @@
             for _, arrived in spreads:
                 arrived(k)
 
-    def send_full(rings):
-        for kind in (0, 1):
-            for copy, _ in rings:
-                go(copy(kind))
-
     def send_tokens(k):
         go(remote(tok.at[x_peers[k][1]], X.at[pl.ds(64, 64), cols(x, 256)], st.at[k], rt.at[k], x_peers[k]))
 
@@ -154,12 +148,13 @@
     send_spread(spreads1[1])
     for k in (1, 0, 2):
         send_tokens(k)
+    for k in (1, 0, 2):
+        send_parameters(k)
     end_spread(spreads1[0])
     send_spread(spreads2[0])
     end_spread(spreads1[1])
     send_spread(spreads2[1])
-    for k in (1, 0, 2):
-        send_parameters(k)
+    send_spread(spreads2[2])
     for k in range(3):
         part = X.at[pl.ds(64, 64), cols(wrap(x - (k + 1), 4), 256)]
         remote(part, part, st.at[k], rt.at[k], x_peers[k]).wait_recv()
@@ -182,50 +177,65 @@
                 part = region(l, 1, p, at, 1 - c, half)
                 remote(part, part, sd.at[l, p, kind], rd.at[l, p, kind], partner).wait_recv()
 
-    def full3(l):
-        send_full(rings3[l])
+    def first3(l):
+        for kind in (0, 1):
+            for copy, _ in rings3[l]:
+                go(copy(kind))
+
+    def second3(l):
+        for kind in (2, 3):
+            for copy, _ in rings3[l]:
+                go(copy(kind))
         for p in range(3):
             hand(l, p, 0)
 
     def forward3(l):
         for kind in (0, 1):
-            for p, (copy, arrived) in enumerate(rings3[l]):
+            for copy, arrived in rings3[l]:
                 arrived(kind)
-                go(copy(kind + 2))
-                hand(l, p, kind + 1)
-
-    def finish3(l):
+                go(copy(kind + 4))
+
+    def planes3(l):
         for kind in (2, 3):
             for p, (_, arrived) in enumerate(rings3[l]):
                 arrived(kind)
-                hand(l, p, kind + 1)
-
-    end_spread(spreads2[0])
-    full3(0)
-    handed(0, (0,))
-    go(remote(core_rows, far, sh.at[1], rh.at[1], across))
-    end_spread(spreads2[1])
-    full3(1)
-    forward3(0)
-    full3(2)
-
-    for k in range(3):
-        origin = wrap(x - (k + 1), 4)
-        part = T.at[origin, share]
-        remote(part, part, sp_.at[0, k], rp_.at[0, k], x_peers[k]).wait_recv()
-        go(remote(part, part, sp_.at[1, k], rp_.at[1, k], partner))
+                hand(l, p, kind - 1)
+
+    def finish3(l):
+        for kind in (4, 5):
+            for p, (_, arrived) in enumerate(rings3[l]):
+                arrived(kind)
+                hand(l, p, kind - 1)
+
+    def parameters():
+        for k in range(3):
+            part = T.at[wrap(x - (k + 1), 4), share]
+            remote(part, part, sp_.at[0, k], rp_.at[0, k], x_peers[k]).wait_recv()
+            go(remote(part, part, sp_.at[1, k], rp_.at[1, k], partner))
+
+    def parameters_here():
+        for k in range(3):
+            part = T.at[wrap(x - (k + 1), 4), pl.ds(17 - 17 * c, 17)]
+            remote(part, part, sp_.at[1, k], rp_.at[1, k], partner).wait_recv()
+
+    def halo_across():
+        handed(0, (0,))
+        go(remote(core_rows, far, sh.at[1], rh.at[1], across))
+
+    def halo_here():
+        remote(core_rows, far, sh.at[0], rh.at[0], partner).wait_recv()
+        remote(core_rows, near, sh.at[1], rh.at[1], across).wait_recv()
 
     def norm(l):
         low, rows = STEP * l, 192 - 2 * STEP * l
         src = X if l == 0 else Y
         g = gainv[l : l + 1, :]
 
-        @pl.loop(0, rows // 16)
-        def _(i):
-            r = pl.multiple_of(low + i * 16, 16)
-            v = src[pl.ds(r, 16), :].astype(F32)
+        for r in range(low, low + rows, NORM_CHUNK):
+            at = pl.ds(r, NORM_CHUNK)
+            v = src[at, :].astype(F32)
             scaled = v * lax.rsqrt(jnp.mean(v * v, axis=-1, keepdims=True) + EPSILON)
-            N[pl.ds(r, 16), :] = (scaled * g).astype(BF16)
+            N[at, :] = (scaled * g).astype(BF16)
 
     def project(l, p, dst):
         low, rows = STEP * l, 192 - 2 * STEP * l
@@ -235,13 +245,12 @@
     def gating(l):
         low, rows = STEP * l, 192 - 2 * STEP * l
 
-        @pl.loop(0, rows // 16)
-        def _(i):
-            r = pl.multiple_of(low + i * 16, 16)
-            at = pl.ds(r, 16)
+        for r in range(low, low + rows, CHUNK):
+            at = pl.ds(r, CHUNK)
             g = (V[at, :] * jax.nn.sigmoid(G[at, :])).astype(BF16).astype(F32)
-            where = sp * 64 - 64 + r + lax.broadcasted_iota(jnp.int32, (16, 512), 0)
-            g = jnp.where((where >= 0) & (where < 2048), g, 0.0)
+            if r < 64 or r + CHUNK > 128:
+                where = sp * 64 - 64 + r + lax.broadcasted_iota(jnp.int32, (CHUNK, 512), 0)
+                g = jnp.where((where >= 0) & (where < 2048), g, 0.0)
             for j in range(4):
                 GT[j, at, :] = g[:, 128 * j : 128 * j + 128]
 
@@ -259,9 +268,8 @@
         g = jnp.concatenate([T[j, TAPS + 1, l : l + 1, :] for j in range(4)], axis=1)
         b = jnp.concatenate([T[j, TAPS + 2, l : l + 1, :] for j in range(4)], axis=1)
 
-        @pl.loop(0, rows // 16)
-        def _(i):
-            at = pl.ds(pl.multiple_of(low + i * 16, 16), 16)
+        for r in range(low, low + rows, CHUNK):
+            at = pl.ds(r, CHUNK)
             v = CV[at, :]
             centered = v - jnp.mean(v, axis=-1, keepdims=True)
             spread = jnp.mean(centered * centered, axis=-1, keepdims=True)
@@ -283,39 +291,59 @@
             else:
                 O[q] = total
 
-    def compute(l, between=()):
-        steps = [
-            functools.partial(norm, l),
-            functools.partial(project, l, 0, V),
-            functools.partial(project, l, 1, G),
-            functools.partial(gating, l),
-            functools.partial(conv, l),
-            functools.partial(channel_norm, l),
-            functools.partial(output, l),
-        ]
-        between = dict(between)
-        for i, step in enumerate(steps):
-            if i in between:
-                between[i]()
-            step()
-
+    def compute(l, first=0, last=7):
+        steps = (
+            norm,
+            lambda l: project(l, 0, V),
+            lambda l: project(l, 1, G),
+            gating,
+            conv,
+            channel_norm,
+            output,
+        )
+        for step in steps[first:last]:
+            step(l)
+
+    end_spread(spreads2[0])
+    first3(0)
+    second3(0)
+    halo_across()
+    end_spread(spreads2[1])
+    first3(1)
+    second3(1)
+    parameters()
+    end_spread(spreads2[2])
+    forward3(0)
+    first3(2)
+    first3(3)
+    planes3(0)
     forward3(1)
+    second3(2)
+    planes3(1)
     finish3(0)
-    full3(3)
+    halo_here()
+    norm(0)
+    forward3(2)
+    second3(3)
+    parameters_here()
     handed(0, (1, 2, 3, 4))
-    for k in range(3):
-        origin = wrap(x - (k + 1), 4)
-        part = T.at[origin, pl.ds(17 - 17 * c, 17)]
-        remote(part, part, sp_.at[1, k], rp_.at[1, k], partner).wait_recv()
-    remote(core_rows, far, sh.at[0], rh.at[0], partner).wait_recv()
-    remote(core_rows, near, sh.at[1], rh.at[1], across).wait_recv()
-    compute(0, {3: lambda: forward3(2), 5: lambda: finish3(1)})
+    compute(0, 1, 4)
+    forward3(3)
+    compute(0, 4, 7)
+    finish3(1)
+    planes3(2)
     handed(1)
-    compute(1, {3: lambda: forward3(3), 5: lambda: finish3(2)})
+    compute(1, 0, 3)
+    finish3(2)
+    compute(1, 3, 7)
+    planes3(3)
     handed(2)
-    compute(2, {5: lambda: finish3(3)})
+    compute(2, 0, 3)
+    finish3(3)
+    compute(2, 3, 7)
+    norm(3)
     handed(3)
-    compute(3)
+    compute(3, 1, 7)
 
     mine = pltpu.make_async_copy(O.at[x], out.at[x], loc.at[10])
     mine.start()
@@ -354,8 +382,8 @@
             vmem((4, TAPS + 3, LAYERS, 128), F32),
             dma((11,)),
             dma((2, 3, 3)), dma((2, 3, 3)),
-            dma((2, 3, 3)), dma((2, 3, 3)),
-            dma((LAYERS, 3, 4)), dma((LAYERS, 3, 4)),
+            dma((3, 3, 3)), dma((3, 3, 3)),
+            dma((LAYERS, 3, 6)), dma((LAYERS, 3, 6)),
             dma((LAYERS, 3, 5)), dma((LAYERS, 3, 5)),
             dma((3,)), dma((3,)),
             dma((2,)), dma((2,)),

time: 54.3 us -> 49.1 us (0.904)
  Pallas kernels: 52.6 us -> 47.4 us
    pallas_call x1, Pallas kernels: 52.6 us -> 47.4 us  [shards(): pl.pallas_call(kernel, name='conv_stack', out_shape=jax.ShapeDtypeStruct(...]
where the time goes in v5:
time: 49.1 us; the launch traced here: 49 us
  Pallas kernels  47.4 us (97%)
  local copies, waits for them, and re-layouts  1.57 us (3%)
    pallas_call x1, Pallas kernels, shards(): pl.pallas_call(kernel, name='conv_stack', out_shape=jax.ShapeDtypeStruct(...  47.4 us
    unnamed x1, local copies, waits for them, and re-layouts  1.57 us

profile of v5, /device:TPU:1, one launch (start us, length us, event | category | flops | bytes accessed | tf_op | source)
XLA Modules:
  0.0 49.0 jit_solution(13160472124893491802)
XLA Ops:
  0.0 47.4 %conv_stack.1 = bf16[4,64,256]{2,1,0:T(8,128)(2,1)} custom-call(bf16[4,64,256]{2,1,0:T(8,128)(2,1)} %tok.1, f32[4,1024]{1,0:T(4,128)} %gain.1, bf16[4,32,128]{2,1,0:T(8,128)(2,1)} %val.1, bf16[4,32,128]{2,1,0:T(8,128)(2,1)} %gate.1, f32[31,4,128]{2,1,0:T(4,128)} %bitcast.2, f32[4,128]{1,0:T(4,128)} %bias.1, f32[4,128]{1,0:T(4,128)} %lng.1, f32[4,128]{1,0:T(4,128)} %lnb.1, ...), custom_call_target="tpu_custom_call" | custom-call | tf_op jit(solution)/shard_map/conv_stack/pallas_call | solution.py:364
  47.4 1.6 %copy.11 = bf16[4,64,256]{2,1,0:T(8,128)(2,1)} copy(bf16[4,64,256]{2,1,0:T(8,128)(2,1)} %conv_stack.1) | data formatting | bytes 262144

commit v6 on v5

--- a/solution.py
+++ b/solution.py
@@ -169,10 +169,10 @@
         part = region(l, 1, p, at, c, half)
         go(remote(part, part, sd.at[l, p, kind], rd.at[l, p, kind], partner))
 
-    def handed(l, kinds=(0, 1, 2, 3, 4)):
+    def handed(l, kinds=(0, 1, 2, 3, 4), parts=(0, 1, 2)):
         for kind in kinds:
             step, half = ((0, None), (1, None), (-1, None), (2, 0), (2, 1))[kind]
-            for p in range(3):
+            for p in parts:
                 at = held(p, 2, wrap(me[ORDERS[p][2]] - step, 4))
                 part = region(l, 1, p, at, 1 - c, half)
                 remote(part, part, sd.at[l, p, kind], rd.at[l, p, kind], partner).wait_recv()
@@ -326,24 +326,36 @@
     forward3(2)
     second3(3)
     parameters_here()
-    handed(0, (1, 2, 3, 4))
+    handed(0, (1, 2, 3, 4), (0, 1))
     compute(0, 1, 4)
     forward3(3)
-    compute(0, 4, 7)
+    compute(0, 4, 6)
+    handed(0, (1, 2, 3, 4), (2,))
+    compute(0, 6, 7)
     finish3(1)
     planes3(2)
-    handed(1)
-    compute(1, 0, 3)
+    norm(1)
+    handed(1, parts=(0, 1))
+    compute(1, 1, 3)
     finish3(2)
-    compute(1, 3, 7)
+    compute(1, 3, 6)
+    handed(1, parts=(2,))
+    compute(1, 6, 7)
     planes3(3)
-    handed(2)
-    compute(2, 0, 3)
+    norm(2)
+    handed(2, parts=(0, 1))
+    compute(2, 1, 3)
     finish3(3)
-    compute(2, 3, 7)
+    compute(2, 3, 6)
+    handed(2, parts=(2,))
+    compute(2, 6, 7)
     norm(3)
-    handed(3)
-    compute(3, 1, 7)
+    handed(3, parts=(0,))
+    compute(3, 1, 2)
+    handed(3, parts=(1,))
+    compute(3, 2, 6)
+    handed(3, parts=(2,))
+    compute(3, 6, 7)
 
     mine = pltpu.make_async_copy(O.at[x], out.at[x], loc.at[10])
     mine.start()

time: 49.1 us -> 49.6 us (1.010)
  Pallas kernels: 47.4 us -> 47.9 us
    pallas_call x1, Pallas kernels: 47.4 us -> 47.9 us  [shards(): pl.pallas_call(kernel, name='conv_stack', out_shape=jax.ShapeDtypeStruct(...]
where the time goes in v6:
time: 49.6 us; the launch traced here: 49.5 us
  Pallas kernels  47.9 us (97%)
  local copies, waits for them, and re-layouts  1.57 us (3%)
    pallas_call x1, Pallas kernels, shards(): pl.pallas_call(kernel, name='conv_stack', out_shape=jax.ShapeDtypeStruct(...  47.9 us
    unnamed x1, local copies, waits for them, and re-layouts  1.57 us

profile of v6, /device:TPU:1, one launch (start us, length us, event | category | flops | bytes accessed | tf_op | source)
XLA Modules:
  0.0 49.5 jit_solution(3584170690017517732)
XLA Ops:
  0.0 47.9 %conv_stack.1 = bf16[4,64,256]{2,1,0:T(8,128)(2,1)} custom-call(bf16[4,64,256]{2,1,0:T(8,128)(2,1)} %tok.1, f32[4,1024]{1,0:T(4,128)} %gain.1, bf16[4,32,128]{2,1,0:T(8,128)(2,1)} %val.1, bf16[4,32,128]{2,1,0:T(8,128)(2,1)} %gate.1, f32[31,4,128]{2,1,0:T(4,128)} %bitcast.2, f32[4,128]{1,0:T(4,128)} %bias.1, f32[4,128]{1,0:T(4,128)} %lng.1, f32[4,128]{1,0:T(4,128)} %lnb.1, ...), custom_call_target="tpu_custom_call" | custom-call | tf_op jit(solution)/shard_map/conv_stack/pallas_call | solution.py:376
  47.9 1.6 %copy.11 = bf16[4,64,256]{2,1,0:T(8,128)(2,1)} copy(bf16[4,64,256]{2,1,0:T(8,128)(2,1)} %conv_stack.1) | data formatting | bytes 262144

commit v7 on v5

--- a/solution.py
+++ b/solution.py
@@ -357,11 +357,23 @@
         copy.wait_send()
 
 
+def carry(src, dst, held, inward, outward):
+    ins = [pltpu.make_async_copy(src.at[i], held.at[i], inward.at[i]) for i in range(4)]
+    outs = [pltpu.make_async_copy(held.at[i], dst.at[i], outward.at[i]) for i in range(4)]
+    for copy in ins:
+        copy.start()
+    for i, copy in enumerate(ins):
+        copy.wait()
+        outs[i].start()
+    for copy in outs:
+        copy.wait()
+
+
 def shards(tokens, norm_gain, val_weight, gate_weight, conv_taps, conv_bias, ln_gain, ln_shift, out_weight):
     any_ = pl.BlockSpec(memory_space=pltpu.HBM)
     dma = pltpu.SemaphoreType.DMA
     vmem = pltpu.VMEM
-    return pl.pallas_call(
+    result = pl.pallas_call(
         kernel,
         name="conv_stack",
         out_shape=jax.ShapeDtypeStruct(tokens.shape, tokens.dtype),
@@ -397,6 +409,15 @@
         tokens, norm_gain, val_weight, gate_weight, conv_taps.transpose(1, 0, 2), conv_bias, ln_gain, ln_shift,
         out_weight.transpose(0, 2, 1),
     )
+    return pl.pallas_call(
+        carry,
+        name="carry",
+        out_shape=jax.ShapeDtypeStruct(tokens.shape, tokens.dtype),
+        in_specs=[any_],
+        out_specs=any_,
+        scratch_shapes=[vmem(tokens.shape, tokens.dtype), dma((4,)), dma((4,))],
+        compiler_params=pltpu.CompilerParams(vmem_limit_bytes=67043328),
+    )(result)
 
 
 def solution(mesh):

time: 49.1 us -> 49.1 us (level)
  local copies, waits for them, and re-layouts: 1.57 us -> 0 us
  Pallas kernels: 47.4 us -> 48.9 us
    unnamed x1 -> x0, local copies, waits for them, and re-layouts: 1.57 us -> none
    pallas_call x0 -> x1, Pallas kernels: none -> 1.49 us  [shards(): pl.pallas_call(carry, name='carry', out_shape=jax.ShapeDtypeStruct(tokens...]
where the time goes in v7:
time: 49.1 us; the launch traced here: 48.9 us
  Pallas kernels  48.9 us (100%)
    pallas_call x1, Pallas kernels, shards(): pl.pallas_call(kernel, name='conv_stack', out_shape=jax.ShapeDtypeStruct(...  47.4 us
    pallas_call x1, Pallas kernels, shards(): pl.pallas_call(carry, name='carry', out_shape=jax.ShapeDtypeStruct(tokens...  1.49 us

profile of v7, /device:TPU:1, one launch (start us, length us, event | category | flops | bytes accessed | tf_op | source)
XLA Modules:
  0.0 48.9 jit_solution(17446568652128907769)
XLA Ops:
  0.0 47.4 %conv_stack.1.src = bf16[4,64,256]{2,1,0:T(8,128)(2,1)} custom-call(bf16[4,64,256]{2,1,0:T(8,128)(2,1)} %tok.1, f32[4,1024]{1,0:T(4,128)} %gain.1, bf16[4,32,128]{2,1,0:T(8,128)(2,1)} %val.1, bf16[4,32,128]{2,1,0:T(8,128)(2,1)} %gate.1, f32[31,4,128]{2,1,0:T(4,128)} %bitcast.2, f32[4,128]{1,0:T(4,128)} %bias.1, f32[4,128]{1,0:T(4,128)} %lng.1, ...), custom_call_target="tpu_custom_call" | custom-call | tf_op jit(solution)/shard_map/conv_stack/pallas_call | solution.py:376
  47.4 1.5 %carry.1 = bf16[4,64,256]{2,1,0:T(8,128)(2,1)} custom-call(bf16[4,64,256]{2,1,0:T(8,128)(2,1)} %conv_stack.1.src), custom_call_target="tpu_custom_call" | custom-call | tf_op jit(solution)/shard_map/carry/pallas_call | solution.py:412

commit v8 on v5

--- a/solution.py
+++ b/solution.py
@@ -14,7 +14,7 @@
 MESH = pl.DeviceIdType.MESH
 F32, BF16 = jnp.float32, jnp.bfloat16
 ORDERS = (("x", "y", "z"), ("y", "z", "x"), ("z", "x", "y"))
-GROUPS1 = ((0, 1), (1, 3))
+GROUPS1 = ((0, 1), (1, 1), (2, 2))
 GROUPS2 = ((0, 1), (1, 1), (2, 2))
 CHUNK = 32
 NORM_CHUNK = 32
@@ -146,6 +146,7 @@
 
     send_spread(spreads1[0])
     send_spread(spreads1[1])
+    send_spread(spreads1[2])
     for k in (1, 0, 2):
         send_tokens(k)
     for k in (1, 0, 2):
@@ -154,6 +155,7 @@
     send_spread(spreads2[0])
     end_spread(spreads1[1])
     send_spread(spreads2[1])
+    end_spread(spreads1[2])
     send_spread(spreads2[2])
     for k in range(3):
         part = X.at[pl.ds(64, 64), cols(wrap(x - (k + 1), 4), 256)]
@@ -381,7 +383,7 @@
             vmem((LAYERS, 1024), F32),
             vmem((4, TAPS + 3, LAYERS, 128), F32),
             dma((11,)),
-            dma((2, 3, 3)), dma((2, 3, 3)),
+            dma((3, 3, 3)), dma((3, 3, 3)),
             dma((3, 3, 3)), dma((3, 3, 3)),
             dma((LAYERS, 3, 6)), dma((LAYERS, 3, 6)),
             dma((LAYERS, 3, 5)), dma((LAYERS, 3, 5)),

time: 49.1 us -> 49.4 us (level)
  no operation moved by 1% of the time
where the time goes in v8:
time: 49.4 us; the launch traced here: 49.2 us
  Pallas kernels  47.6 us (96%)
  local copies, waits for them, and re-layouts  1.57 us (3%)
    pallas_call x1, Pallas kernels, shards(): pl.pallas_call(kernel, name='conv_stack', out_shape=jax.ShapeDtypeStruct(...  47.6 us
    unnamed x1, local copies, waits for them, and re-layouts  1.57 us

profile of v8, /device:TPU:1, one launch (start us, length us, event | category | flops | bytes accessed | tf_op | source)
XLA Modules:
  0.0 49.2 jit_solution(6645755860709646693)
XLA Ops:
  0.0 47.6 %conv_stack.1 = bf16[4,64,256]{2,1,0:T(8,128)(2,1)} custom-call(bf16[4,64,256]{2,1,0:T(8,128)(2,1)} %tok.1, f32[4,1024]{1,0:T(4,128)} %gain.1, bf16[4,32,128]{2,1,0:T(8,128)(2,1)} %val.1, bf16[4,32,128]{2,1,0:T(8,128)(2,1)} %gate.1, f32[31,4,128]{2,1,0:T(4,128)} %bitcast.2, f32[4,128]{1,0:T(4,128)} %bias.1, f32[4,128]{1,0:T(4,128)} %lng.1, f32[4,128]{1,0:T(4,128)} %lnb.1, ...), custom_call_target="tpu_custom_call" | custom-call | tf_op jit(solution)/shard_map/conv_stack/pallas_call | solution.py:366
  47.6 1.6 %copy.11 = bf16[4,64,256]{2,1,0:T(8,128)(2,1)} copy(bf16[4,64,256]{2,1,0:T(8,128)(2,1)} %conv_stack.1) | data formatting | bytes 262144
